TPU v7x, 32 devices: a whole 2x2x4 slice. The times are simulated.
32 devices in a mesh: sp: 8 (over z, y), tp: 4 (over x, core).
Axes of the slice: x: 2, y: 2, z: 4, core: 2. Of those that a mesh axis runs over, the one named last changes fastest.
Arguments:
- query: bfloat16 [4096, 1024], P('sp', 'tp'), may hold values from -6 to 6
- key: bfloat16 [4096, 1024], P('sp', 'tp'), may hold values from -6 to 6
- value: bfloat16 [4096, 1024], P('sp', 'tp'), may hold values from -6 to 6
- out_grad: bfloat16 [4096, 1024], P('sp', 'tp'), may hold values from -6 to 6
- query_gain: float32 [64], replicated, may hold values from 0.1 to 1.9
- key_gain: float32 [64], replicated, may hold values from 0.1 to 1.9
- rel_bias: float32 [16, 129], P('tp'), may hold values from -3 to 3
Outputs:
- query_grad: bfloat16 [4096, 1024], P('sp', 'tp')
- key_grad: bfloat16 [4096, 1024], P('sp', 'tp')
- value_grad: bfloat16 [4096, 1024], P('sp', 'tp')
- query_gain_grad: float32 [64], replicated
- key_gain_grad: float32 [64], replicated
- bias_grad: float32 [16, 129], P('tp')
All inputs are finite; a program needn't handle non-finite values.
Results may differ from a plain program's by a relative error of at most 0.0095.
Values may be sent and summed in bfloat16 or wider, within the bound.
No kernel may reach another device: no remote copies, remote signals or barrier semaphores. Data moves between devices by JAX's collectives and lax.ppermute only.
A program may use at most 64 MiB of HBM per device.

v0:
```python
import jax
import jax.numpy as jnp
from jax import lax
from jax.sharding import PartitionSpec as P

SEG = 64
PREV = 8
CLIP = 128


epsilon = 1e-06


def shifted(block, axis, distance):
    devices = range(lax.axis_size(axis))
    route = [(i - distance, i) for i in devices if i - distance in devices]
    return lax.ppermute(block, axis, route)


def normalize(head_rows, gain_vector):
    widened = head_rows.astype(jnp.float32)
    row_scale = lax.rsqrt(jnp.mean(widened * widened, axis=-1, keepdims=True) + epsilon)
    unit_rows = widened * row_scale
    return (unit_rows, row_scale, (unit_rows * gain_vector).astype(jnp.bfloat16))


def norm_backward(grad_hat, unit_rows, row_scale, gain_vector):
    grad_unit = grad_hat * gain_vector
    inner_mean = jnp.mean(grad_unit * unit_rows, axis=-1, keepdims=True)
    return (
        row_scale * (grad_unit - unit_rows * inner_mean),
        jnp.sum(grad_hat * unit_rows, axis=(0, 1)),
    )


def bias_matrix(table_row, block):
    tap_count = table_row.shape[0]
    position = jnp.arange(3 * block - 1, dtype=jnp.int32)
    distance = jnp.clip(2 * block - 1 - position, 0, tap_count - 1)
    selected = distance[:, None] == jnp.arange(tap_count, dtype=jnp.int32)[None, :]
    diagonal = jnp.sum(
        jnp.where(selected, table_row[None, :], jnp.zeros((), table_row.dtype)), axis=1
    )
    diagonal = jnp.concatenate(
        [diagonal[block - 1 :], jnp.zeros((1,), diagonal.dtype), diagonal[: block - 1]]
    )
    flattened = jnp.tile(diagonal, block)[: block * (3 * block - 1)]
    return flattened.reshape(block, 3 * block - 1)[:, : 2 * block]


def tap_totals(score_grad, tap_count):
    block = score_grad.shape[0]
    widened = jnp.pad(score_grad, ((0, 0), (0, block - 1)))
    flattened = jnp.pad(widened.reshape(-1), (0, block))
    columns = jnp.sum(flattened.reshape(block, 3 * block), axis=0)
    near_taps = columns[block - tap_count + 2 : block + 1][::-1]
    return jnp.concatenate([near_taps, (jnp.sum(columns) - jnp.sum(near_taps))[None]])


def band_mask(block):
    row_index = jnp.arange(block, dtype=jnp.int32)[:, None]
    col_index = jnp.arange(2 * block, dtype=jnp.int32)[None, :]
    return (row_index + block >= col_index) & (col_index // SEG >= row_index // SEG)


def block_gradients(
    query_block, key_block, value_block, grad_block, bias_block, allowed, score_scale
):
    scores = (
        jnp.dot(query_block, key_block.T, preferred_element_type=jnp.float32) * score_scale
        + bias_block
    )
    normalizer = jnp.sum(
        jnp.where(allowed, jnp.exp(scores), jnp.zeros((), jnp.float32)), axis=1, keepdims=True
    )
    log_total = jnp.log(normalizer)
    attention = jnp.where(allowed, jnp.exp(scores - log_total), jnp.zeros((), jnp.float32))
    attention_low = attention.astype(jnp.bfloat16)
    output_low = jnp.dot(attention_low, value_block, preferred_element_type=jnp.float32).astype(
        jnp.bfloat16
    )
    output_low = lax.optimization_barrier(output_low)
    row_delta = jnp.sum(
        grad_block.astype(jnp.float32) * output_low.astype(jnp.float32), axis=1, keepdims=True
    )
    attention_grad = jnp.dot(grad_block, value_block.T, preferred_element_type=jnp.float32)
    score_grad = attention * (attention_grad - row_delta)
    score_low = score_grad.astype(jnp.bfloat16)
    query_part = jnp.dot(score_low, key_block, preferred_element_type=jnp.float32) * score_scale
    key_part = jnp.dot(score_low.T, query_block, preferred_element_type=jnp.float32) * score_scale
    value_part = jnp.dot(attention_low.T, grad_block, preferred_element_type=jnp.float32)
    tap_part = tap_totals(score_grad, CLIP + 1)
    return (query_part, key_part, value_part, tap_part, log_total, row_delta)


def per_device(query, key, value, out_grad, query_gain, key_gain, rel_bias):
    block = PREV * SEG
    row_count = query.shape[0]
    local_heads = rel_bias.shape[0]
    head_width = query.shape[1] // local_heads
    score_scale = head_width ** (-0.5)
    shape = (row_count, local_heads, head_width)
    query_unit, query_scale, query_hat = normalize(query.reshape(shape), query_gain)
    key_unit, key_scale, key_hat = normalize(key.reshape(shape), key_gain)
    value_rows = value.reshape(shape)
    grad_rows = out_grad.reshape(shape)
    tail_start = row_count - block
    before_key, before_value = shifted((key_hat, value_rows), "sp", 1)
    key_heads = jnp.concatenate([before_key, key_hat]).transpose(1, 0, 2)
    value_heads = jnp.concatenate([before_value, value_rows]).transpose(1, 0, 2)
    query_heads = query_hat.transpose(1, 0, 2)
    grad_heads = grad_rows.transpose(1, 0, 2)
    inside = band_mask(block)
    later = jnp.arange(2 * block, dtype=jnp.int32)[None, :] >= block
    leading = inside & (later | (lax.axis_index("sp") > 0))

    def per_head(items):
        query_part, key_part, value_part, grad_part, table_row = items
        bias_block = bias_matrix(table_row, block)
        key_total = jnp.zeros((row_count + block, head_width), jnp.float32)
        value_total = jnp.zeros((row_count + block, head_width), jnp.float32)
        first_stats = None
        results = block_gradients(
            query_part, key_part, value_part, grad_part, bias_block, leading, score_scale
        )
        query_pieces = [results[0]]
        key_total = key_total.at[0 : 2 * block].add(results[1])
        value_total = value_total.at[0 : 2 * block].add(results[2])
        tap_total = results[3]
        first_stats = (results[4], results[5])
        return (
            jnp.concatenate(query_pieces),
            key_total,
            value_total,
            tap_total,
            first_stats[0],
            first_stats[1],
            bias_block[:, :block],
        )

    query_hat_grad, key_total, value_total, tap_grads, log_totals, row_deltas, bias_blocks = (
        lax.map(per_head, (query_heads, key_heads, value_heads, grad_heads, rel_bias))
    )
    key_own = key_total[:, block:]
    value_own = value_total[:, block:]
    back_key, back_value = (
        shifted(key_total[:, :block].astype(jnp.bfloat16), "sp", -1).astype(jnp.float32),
        shifted(value_total[:, :block].astype(jnp.bfloat16), "sp", -1).astype(jnp.float32),
    )
    key_own = key_own.at[:, tail_start:].add(back_key)
    value_own = value_own.at[:, tail_start:].add(back_value)
    query_grad, query_gain_part = norm_backward(
        query_hat_grad.transpose(1, 0, 2), query_unit, query_scale, query_gain
    )
    key_grad, key_gain_part = norm_backward(
        key_own.transpose(1, 0, 2), key_unit, key_scale, key_gain
    )
    head_offset = lax.axis_index("tp") * local_heads
    every_head = jnp.zeros((local_heads * lax.axis_size("tp"), tap_grads.shape[1]), jnp.float32)
    every_head = lax.dynamic_update_slice_in_dim(every_head, tap_grads, head_offset, 0)
    every_head, query_gain_grad, key_gain_grad = lax.psum(
        (every_head, query_gain_part, key_gain_part), ("sp", "tp")
    )
    bias_grad = lax.dynamic_slice_in_dim(every_head, head_offset, local_heads, 0)
    flat_width = local_heads * head_width
    value_grad = value_own.transpose(1, 0, 2).reshape(row_count, flat_width)
    return (
        query_grad.reshape(row_count, flat_width).astype(jnp.bfloat16),
        key_grad.reshape(row_count, flat_width).astype(jnp.bfloat16),
        value_grad.astype(jnp.bfloat16),
        query_gain_grad,
        key_gain_grad,
        bias_grad,
    )


def solution(mesh):
    placed = (P("sp", "tp"), P("sp", "tp"), P("sp", "tp"), P("sp", "tp"), P(), P(), P("tp", None))
    return jax.shard_map(
        per_device,
        mesh=mesh,
        in_specs=placed,
        out_specs=(P("sp", "tp"), P("sp", "tp"), P("sp", "tp"), P(), P(), P("tp", None)),
        check_vma=False,
    )
```

profile of v0, /device:TPU:0, one launch (start us, length us, event | category | flops | bytes accessed | tf_op | source)
XLA Modules:
  0.0 205.3 jit_solution(8856687022407626917)
XLA Ops:
  0.7 1.1 copy.32
  1.9 0.9 multiply_convert_fusion.2
  2.9 4.9 %collective-permute-start = (bf16[512,4,64]{0,2,1:T(8,128)(2,1)S(1)}, bf16[512,4,64]{0,2,1:T(8,128)(2,1)S(1)}, u32[]{:S(2)}, u32[]{:S(2)}) collective-permute-start(bf16[512,4,64]{0,2,1:T(8,128)(2,1)S(1)} %multiply_convert_fusion.2), channel_id=1, source_target_pairs={{0,4},{4,8},{8,12},{12,16},{16,20},{20,24},{24,28},{1,5},{5,9},{9,... | collective-permute-start | bytes 786440 | tf_op jit(solution)/shard_map/ppermute | solution.py:17
  7.9 3.4 %collective-permute-start.1 = (bf16[512,4,64]{0,2,1:T(8,128)(2,1)S(1)}, bf16[512,4,64]{0,2,1:T(8,128)(2,1)S(1)}, u32[]{:S(2)}, u32[]{:S(2)}) collective-permute-start(bf16[512,4,64]{0,2,1:T(8,128)(2,1)S(1)} %bitcast.127), channel_id=1, source_target_pairs={{0,4},{4,8},{8,12},{12,16},{16,20},{20,24},{24,28},{1,5},{5,9},{9,... | collective-permute-start | bytes 786440 | tf_op jit(solution)/shard_map/ppermute | solution.py:17
  12.7 1.8 collective-permute-done
  15.3 3.6 %collective-permute-done.1 = bf16[512,4,64]{0,2,1:T(8,128)(2,1)S(1)} collective-permute-done((bf16[512,4,64]{0,2,1:T(8,128)(2,1)S(1)}, bf16[512,4,64]{0,2,1:T(8,128)(2,1)S(1)}, u32[]{:S(2)}, u32[]{:S(2)}) %collective-permute-start.1) | collective-permute-done | bytes 262176 | tf_op jit(solution)/shard_map/ppermute | solution.py:17
  18.9 0.9 maximum_bitcast_fusion.1
  19.8 121.7 %while.28 = (s32[]{:T(128)}, f32[4,512,64]{1,2,0:T(8,128)}, f32[4,1024,64]{1,2,0:T(8,128)}, f32[4,1024,64]{1,2,0:T(8,128)}, f32[4,129]{1,0:T(4,128)S(1)}, /*inde...) while((s32[]{:T(128)}, f32[4,512,64]{1,2,0:T(8,128)}, ...), condition=%wide.region_9.10_spmd.clone, body=%wide.region_2.9_spmd.clone.sunk | while | flops 421858688 | bytes 64660764 | solution.py:142
  21.3 1.9 tile.22
  23.1 4.0 %reshape.313 = f32[512,1535]{1,0:T(8,128)S(1)} reshape(f32[785920]{0:T(1024)} %bitcast.122) | data formatting | bytes 6287360 | tf_op jit(solution)/shard_map/while/body/eval_jaxpr/reshape | solution.py:48
  27.1 2.1 %select_reduce_fusion.5 = (f32[512]{0:T(512)S(1)}, f32[512,1024]{1,0:T(8,128)S(1)}) fusion(pred[1024]{0:T(1024)(128)(4,1)S(1)} %get-tuple-element.540, s32[512]{0:T(512)S(1)} %get-tuple-element.538, s32[1024]{0:T(1024)S(1)} %get-tuple-element.539, s32[512]{0:T(512)S(1)} %get-tuple-element.537, f32[512,1535]{1,0:T(8,128)S(1)} %reshape.313, ...), kind=kOutput, calls=%fused_computation.5.clone.1 | convolution fusion | flops 71302656 | bytes 4403200 | tf_op jit(solution)/shard_map/while/body/eval_jaxpr/dot_general | solution.py:70
  29.3 0.9 convolution_convert_fusion.2
  30.3 1.0 subtract_multiply_fusion.2
  31.3 2.0 fusion.73
  33.3 1.0 fusion.74
  34.4 1.6 fusion.75
  36.0 2.1 %pad.51 = f32[512,1535]{1,0:T(8,128)} pad(f32[512,1024]{1,0:T(8,128)S(1)} %subtract_multiply_fusion.2, f32[]{:T(128)} %constant.259.clone.1..sunk), padding=0_0x0_511 | pad | bytes 5240836 | tf_op jit(solution)/shard_map/while/body/eval_jaxpr/jit(_pad)/pad | solution.py:53
  38.0 4.0 %reshape.314 = f32[785920]{0:T(1024)S(1)} reshape(f32[512,1535]{1,0:T(8,128)} %pad.51) | data formatting | bytes 6287360 | tf_op jit(solution)/shard_map/while/body/eval_jaxpr/reshape | solution.py:54
  42.1 3.0 %fusion.76 = (f32[786432]{0:T(1024)}, f32[]{:T(128)}) fusion(f32[785920]{0:T(1024)S(1)} %reshape.314), kind=kLoop, calls=%fused_computation.93.clone.1 | loop fusion | flops 786431 | bytes 6289412 | tf_op jit(solution)/shard_map/while/body/eval_jaxpr/jit(_pad)/pad | solution.py:54
  45.1 2.8 %reshape.315 = f32[512,1536]{1,0:T(8,128)S(1)} reshape(f32[786432]{0:T(1024)} %get-tuple-element.490) | data formatting | bytes 6291456 | tf_op jit(solution)/shard_map/while/body/eval_jaxpr/reshape | solution.py:55
  51.7 1.9 tile.22
  53.6 4.0 %reshape.313 = f32[512,1535]{1,0:T(8,128)S(1)} reshape(f32[785920]{0:T(1024)} %bitcast.122) | data formatting | bytes 6287360 | tf_op jit(solution)/shard_map/while/body/eval_jaxpr/reshape | solution.py:48
  57.6 2.1 %select_reduce_fusion.5 = (f32[512]{0:T(512)S(1)}, f32[512,1024]{1,0:T(8,128)S(1)}) fusion(pred[1024]{0:T(1024)(128)(4,1)S(1)} %get-tuple-element.540, s32[512]{0:T(512)S(1)} %get-tuple-element.538, s32[1024]{0:T(1024)S(1)} %get-tuple-element.539, s32[512]{0:T(512)S(1)} %get-tuple-element.537, f32[512,1535]{1,0:T(8,128)S(1)} %reshape.313, ...), kind=kOutput, calls=%fused_computation.5.clone.1 | convolution fusion | flops 71302656 | bytes 4403200 | tf_op jit(solution)/shard_map/while/body/eval_jaxpr/dot_general | solution.py:70
  59.7 0.9 convolution_convert_fusion.2
  60.7 1.0 subtract_multiply_fusion.2
  61.7 2.0 fusion.73
  63.8 1.0 fusion.74
  64.8 1.6 fusion.75
  66.4 2.1 %pad.51 = f32[512,1535]{1,0:T(8,128)} pad(f32[512,1024]{1,0:T(8,128)S(1)} %subtract_multiply_fusion.2, f32[]{:T(128)} %constant.259.clone.1..sunk), padding=0_0x0_511 | pad | bytes 5240836 | tf_op jit(solution)/shard_map/while/body/eval_jaxpr/jit(_pad)/pad | solution.py:53
  68.5 4.0 %reshape.314 = f32[785920]{0:T(1024)S(1)} reshape(f32[512,1535]{1,0:T(8,128)} %pad.51) | data formatting | bytes 6287360 | tf_op jit(solution)/shard_map/while/body/eval_jaxpr/reshape | solution.py:54
  72.5 3.0 %fusion.76 = (f32[786432]{0:T(1024)}, f32[]{:T(128)}) fusion(f32[785920]{0:T(1024)S(1)} %reshape.314), kind=kLoop, calls=%fused_computation.93.clone.1 | loop fusion | flops 786431 | bytes 6289412 | tf_op jit(solution)/shard_map/while/body/eval_jaxpr/jit(_pad)/pad | solution.py:54
  75.5 2.8 %reshape.315 = f32[512,1536]{1,0:T(8,128)S(1)} reshape(f32[786432]{0:T(1024)} %get-tuple-element.490) | data formatting | bytes 6291456 | tf_op jit(solution)/shard_map/while/body/eval_jaxpr/reshape | solution.py:55
  82.1 1.9 tile.22
  84.0 4.0 %reshape.313 = f32[512,1535]{1,0:T(8,128)S(1)} reshape(f32[785920]{0:T(1024)} %bitcast.122) | data formatting | bytes 6287360 | tf_op jit(solution)/shard_map/while/body/eval_jaxpr/reshape | solution.py:48
  88.0 2.1 %select_reduce_fusion.5 = (f32[512]{0:T(512)S(1)}, f32[512,1024]{1,0:T(8,128)S(1)}) fusion(pred[1024]{0:T(1024)(128)(4,1)S(1)} %get-tuple-element.540, s32[512]{0:T(512)S(1)} %get-tuple-element.538, s32[1024]{0:T(1024)S(1)} %get-tuple-element.539, s32[512]{0:T(512)S(1)} %get-tuple-element.537, f32[512,1535]{1,0:T(8,128)S(1)} %reshape.313, ...), kind=kOutput, calls=%fused_computation.5.clone.1 | convolution fusion | flops 71302656 | bytes 4403200 | tf_op jit(solution)/shard_map/while/body/eval_jaxpr/dot_general | solution.py:70
  90.1 0.9 convolution_convert_fusion.2
  91.1 1.0 subtract_multiply_fusion.2
  92.2 2.0 fusion.73
  94.2 1.0 fusion.74
  95.2 1.6 fusion.75
  96.8 2.1 %pad.51 = f32[512,1535]{1,0:T(8,128)} pad(f32[512,1024]{1,0:T(8,128)S(1)} %subtract_multiply_fusion.2, f32[]{:T(128)} %constant.259.clone.1..sunk), padding=0_0x0_511 | pad | bytes 5240836 | tf_op jit(solution)/shard_map/while/body/eval_jaxpr/jit(_pad)/pad | solution.py:53
  98.9 4.0 %reshape.314 = f32[785920]{0:T(1024)S(1)} reshape(f32[512,1535]{1,0:T(8,128)} %pad.51) | data formatting | bytes 6287360 | tf_op jit(solution)/shard_map/while/body/eval_jaxpr/reshape | solution.py:54
  102.9 3.0 %fusion.76 = (f32[786432]{0:T(1024)}, f32[]{:T(128)}) fusion(f32[785920]{0:T(1024)S(1)} %reshape.314), kind=kLoop, calls=%fused_computation.93.clone.1 | loop fusion | flops 786431 | bytes 6289412 | tf_op jit(solution)/shard_map/while/body/eval_jaxpr/jit(_pad)/pad | solution.py:54
  105.9 2.8 %reshape.315 = f32[512,1536]{1,0:T(8,128)S(1)} reshape(f32[786432]{0:T(1024)} %get-tuple-element.490) | data formatting | bytes 6291456 | tf_op jit(solution)/shard_map/while/body/eval_jaxpr/reshape | solution.py:55
  112.5 1.9 tile.22
  114.4 4.0 %reshape.313 = f32[512,1535]{1,0:T(8,128)S(1)} reshape(f32[785920]{0:T(1024)} %bitcast.122) | data formatting | bytes 6287360 | tf_op jit(solution)/shard_map/while/body/eval_jaxpr/reshape | solution.py:48
  118.4 2.1 %select_reduce_fusion.5 = (f32[512]{0:T(512)S(1)}, f32[512,1024]{1,0:T(8,128)S(1)}) fusion(pred[1024]{0:T(1024)(128)(4,1)S(1)} %get-tuple-element.540, s32[512]{0:T(512)S(1)} %get-tuple-element.538, s32[1024]{0:T(1024)S(1)} %get-tuple-element.539, s32[512]{0:T(512)S(1)} %get-tuple-element.537, f32[512,1535]{1,0:T(8,128)S(1)} %reshape.313, ...), kind=kOutput, calls=%fused_computation.5.clone.1 | convolution fusion | flops 71302656 | bytes 4403200 | tf_op jit(solution)/shard_map/while/body/eval_jaxpr/dot_general | solution.py:70
  120.6 0.9 convolution_convert_fusion.2
  121.6 1.0 subtract_multiply_fusion.2
  122.6 2.0 fusion.73
  124.6 1.0 fusion.74
  125.6 1.7 fusion.75
  127.3 2.1 %pad.51 = f32[512,1535]{1,0:T(8,128)} pad(f32[512,1024]{1,0:T(8,128)S(1)} %subtract_multiply_fusion.2, f32[]{:T(128)} %constant.259.clone.1..sunk), padding=0_0x0_511 | pad | bytes 5240836 | tf_op jit(solution)/shard_map/while/body/eval_jaxpr/jit(_pad)/pad | solution.py:53
  129.3 4.0 %reshape.314 = f32[785920]{0:T(1024)S(1)} reshape(f32[512,1535]{1,0:T(8,128)} %pad.51) | data formatting | bytes 6287360 | tf_op jit(solution)/shard_map/while/body/eval_jaxpr/reshape | solution.py:54
  133.4 3.0 %fusion.76 = (f32[786432]{0:T(1024)}, f32[]{:T(128)}) fusion(f32[785920]{0:T(1024)S(1)} %reshape.314), kind=kLoop, calls=%fused_computation.93.clone.1 | loop fusion | flops 786431 | bytes 6289412 | tf_op jit(solution)/shard_map/while/body/eval_jaxpr/jit(_pad)/pad | solution.py:54
  136.4 2.8 %reshape.315 = f32[512,1536]{1,0:T(8,128)S(1)} reshape(f32[786432]{0:T(1024)} %get-tuple-element.490) | data formatting | bytes 6291456 | tf_op jit(solution)/shard_map/while/body/eval_jaxpr/reshape | solution.py:55
  141.6 1.9 fusion.39
  143.5 1.8 slice.143
  145.2 1.3 collective-permute-start.2
  147.6 1.3 collective-permute-start.3
  148.9 8.1 %collective-permute-done.2 = bf16[4,512,64]{1,2,0:T(8,128)(2,1)S(1)} collective-permute-done((bf16[4,512,64]{1,2,0:T(8,128)(2,1)}, bf16[4,512,64]{1,2,0:T(8,128)(2,1)S(1)}, u32[]{:S(2)}, u32[]{:S(2)}) %collective-permute-start.2) | collective-permute-done | bytes 262176 | tf_op jit(solution)/shard_map/ppermute | solution.py:17
  158.3 2.7 %collective-permute-done.3 = bf16[4,512,64]{1,2,0:T(8,128)(2,1)} collective-permute-done((bf16[4,512,64]{1,2,0:T(8,128)(2,1)S(1)}, bf16[4,512,64]{1,2,0:T(8,128)(2,1)}, u32[]{:S(2)}, u32[]{:S(2)}) %collective-permute-start.3) | collective-permute-done | bytes 262176 | tf_op jit(solution)/shard_map/ppermute | solution.py:17
  161.0 1.0 add_convert_fusion
  162.9 41.8 %all-reduce.2 = (f32[64]{0:T(128)}, f32[64]{0:T(128)}, f32[16,129]{1,0:T(8,128)S(1)}) all-reduce(f32[64]{0:T(128)S(1)} %get-tuple-element.359, f32[64]{0:T(128)S(1)} %get-tuple-element.357, f32[16,129]{1,0:T(8,128)S(1)} %constant_dynamic-update-slice_fusion), channel_id=1, replica_groups=mesh['sp'=8,'tp'=4] {'sp','tp'}, use_global_device_ids=true, to_apply=%region_13.14 | all-reduce | flops 2192 | bytes 17536 | tf_op jit(solution)/shard_map/psum | solution.py:161
  (128 shorter events, 16.1 us)
Async XLA Ops:
  0.6 7.1 %copy-start.10 = (bf16[512,256]{1,0:T(8,128)(2,1)S(1)}, bf16[512,256]{1,0:T(8,128)(2,1)}, u32[]{:S(2)}) copy-start(bf16[512,256]{1,0:T(8,128)(2,1)} %param.27) | copy-start | bytes 786436
  0.6 10.7 %copy-start.9 = (bf16[512,256]{1,0:T(8,128)(2,1)S(1)}, bf16[512,256]{1,0:T(8,128)(2,1)}, u32[]{:S(2)}) copy-start(bf16[512,256]{1,0:T(8,128)(2,1)} %param.25) | copy-start | bytes 786436
  0.7 11.0 %copy-start.12 = (f32[64]{0:T(128)S(1)}, f32[64]{0:T(128)}, u32[]{:S(2)}) copy-start(f32[64]{0:T(128)} %param.29) | copy-start | bytes 772
  1.8 10.8 %copy-start = (f32[512,256]{0,1:T(8,128)}, f32[512,256]{0,1:T(8,128)S(1)}, u32[]{:S(2)}) copy-start(f32[512,256]{0,1:T(8,128)S(1)} %copy.32) | copy-start | bytes 1572868
  1.8 10.0 %copy-start.11 = (bf16[512,256]{1,0:T(8,128)(2,1)S(1)}, bf16[512,256]{1,0:T(8,128)(2,1)}, u32[]{:S(2)}) copy-start(bf16[512,256]{1,0:T(8,128)(2,1)} %param.28) | copy-start | bytes 786436
  2.9 11.6 %collective-permute-start = (bf16[512,4,64]{0,2,1:T(8,128)(2,1)S(1)}, bf16[512,4,64]{0,2,1:T(8,128)(2,1)S(1)}, u32[]{:S(2)}, u32[]{:S(2)}) collective-permute-start(bf16[512,4,64]{0,2,1:T(8,128)(2,1)S(1)} %multiply_convert_fusion.2), channel_id=1, source_target_pairs={{0,4},{4,8},{8,12},{12,16},{16,20},{20,24},{24,28},{1,5},{5,9},{9,... | collective-permute-start | bytes 786440 | tf_op jit(solution)/shard_map/ppermute | solution.py:17
  7.9 11.0 %collective-permute-start.1 = (bf16[512,4,64]{0,2,1:T(8,128)(2,1)S(1)}, bf16[512,4,64]{0,2,1:T(8,128)(2,1)S(1)}, u32[]{:S(2)}, u32[]{:S(2)}) collective-permute-start(bf16[512,4,64]{0,2,1:T(8,128)(2,1)S(1)} %bitcast.127), channel_id=1, source_target_pairs={{0,4},{4,8},{8,12},{12,16},{16,20},{20,24},{24,28},{1,5},{5,9},{9,... | collective-permute-start | bytes 786440 | tf_op jit(solution)/shard_map/ppermute | solution.py:17
  11.5 8.3 %copy-start.2 = (f32[512,256]{0,1:T(8,128)}, f32[512,256]{0,1:T(8,128)S(1)}, u32[]{:S(2)}) copy-start(f32[512,256]{0,1:T(8,128)S(1)} %copy.31) | copy-start | bytes 1572868
  27.1 2.2 %copy-start.8 = (bf16[4,1024,64]{1,2,0:T(8,128)(2,1)S(1)}, bf16[4,1024,64]{1,2,0:T(8,128)(2,1)}, u32[]{:S(2)}) copy-start(bf16[4,1024,64]{1,2,0:T(8,128)(2,1)} %get-tuple-element.536) | copy-start | bytes 1572868 | tf_op jit(solution)/shard_map/while
  29.3 1.0 copy-start.6
  57.5 2.2 %copy-start.8 = (bf16[4,1024,64]{1,2,0:T(8,128)(2,1)S(1)}, bf16[4,1024,64]{1,2,0:T(8,128)(2,1)}, u32[]{:S(2)}) copy-start(bf16[4,1024,64]{1,2,0:T(8,128)(2,1)} %get-tuple-element.536) | copy-start | bytes 1572868 | tf_op jit(solution)/shard_map/while
  59.7 1.0 copy-start.6
  88.0 2.2 %copy-start.8 = (bf16[4,1024,64]{1,2,0:T(8,128)(2,1)S(1)}, bf16[4,1024,64]{1,2,0:T(8,128)(2,1)}, u32[]{:S(2)}) copy-start(bf16[4,1024,64]{1,2,0:T(8,128)(2,1)} %get-tuple-element.536) | copy-start | bytes 1572868 | tf_op jit(solution)/shard_map/while
  90.1 1.0 copy-start.6
  118.4 2.2 %copy-start.8 = (bf16[4,1024,64]{1,2,0:T(8,128)(2,1)S(1)}, bf16[4,1024,64]{1,2,0:T(8,128)(2,1)}, u32[]{:S(2)}) copy-start(bf16[4,1024,64]{1,2,0:T(8,128)(2,1)} %get-tuple-element.536) | copy-start | bytes 1572868 | tf_op jit(solution)/shard_map/while
  120.6 1.0 copy-start.6
  141.5 5.0 %copy-start.3 = (f32[512,256]{0,1:T(8,128)S(1)}, f32[512,256]{0,1:T(8,128)}, u32[]{:S(2)}) copy-start(f32[512,256]{0,1:T(8,128)} %copy-done.2) | copy-start | bytes 1572868
  141.5 5.0 %copy-start.4 = (f32[4,512,64]{1,2,0:T(8,128)S(1)}, f32[4,512,64]{1,2,0:T(8,128)}, u32[]{:S(2)}) copy-start(f32[4,512,64]{1,2,0:T(8,128)} %get-tuple-element.265) | copy-start | bytes 1572868
  141.5 6.0 %copy-start.7 = (f32[4,1024,64]{1,2,0:T(8,128)S(1)}, f32[4,1024,64]{1,2,0:T(8,128)}, u32[]{:S(2)}) copy-start(f32[4,1024,64]{1,2,0:T(8,128)} %get-tuple-element.267) | copy-start | bytes 3145732
  141.6 15.4 %copy-start.1 = (f32[512,256]{0,1:T(8,128)S(1)}, f32[512,256]{0,1:T(8,128)}, u32[]{:S(2)}) copy-start(f32[512,256]{0,1:T(8,128)} %copy-done) | copy-start | bytes 1572868
  141.6 15.4 %copy-start.5 = (f32[4,1024,64]{1,2,0:T(8,128)S(1)}, f32[4,1024,64]{1,2,0:T(8,128)}, u32[]{:S(2)}) copy-start(f32[4,1024,64]{1,2,0:T(8,128)} %get-tuple-element.266) | copy-start | bytes 3145732
  141.6 15.4 %copy-start.13 = (f32[64]{0:T(128)S(1)}, f32[64]{0:T(128)}, u32[]{:S(2)}) copy-start(f32[64]{0:T(128)} %param.30) | copy-start | bytes 772
  145.2 11.7 %collective-permute-start.2 = (bf16[4,512,64]{1,2,0:T(8,128)(2,1)}, bf16[4,512,64]{1,2,0:T(8,128)(2,1)S(1)}, u32[]{:S(2)}, u32[]{:S(2)}) collective-permute-start(bf16[4,512,64]{1,2,0:T(8,128)(2,1)} %slice.143), channel_id=1, source_target_pairs={{4,0},{8,4},{12,8},{16,12},{20,16},{24,20},{28,24},{5,1},{9,5},{13... | collective-permute-start | bytes 786440 | tf_op jit(solution)/shard_map/ppermute | solution.py:17
  147.6 13.4 %collective-permute-start.3 = (bf16[4,512,64]{1,2,0:T(8,128)(2,1)S(1)}, bf16[4,512,64]{1,2,0:T(8,128)(2,1)}, u32[]{:S(2)}, u32[]{:S(2)}) collective-permute-start(bf16[4,512,64]{1,2,0:T(8,128)(2,1)S(1)} %slice.142), channel_id=1, source_target_pairs={{4,0},{8,4},{12,8},{16,12},{20,16},{24,20},{28,24},{5,1},{9,5},{13... | collective-permute-start | bytes 786440 | tf_op jit(solution)/shard_map/ppermute | solution.py:17
where the time goes:
time: 207 us; the launch traced here: 205 us
  local copies, waits for them, and re-layouts  72.1 us (35%)
  blocking collectives  41.8 us (20%)
  matrix products  35 us (17%)
  other arithmetic  22.7 us (11%)
  waiting for transfers between devices  16.1 us (8%)
  starting transfers between devices  10.9 us (5%)
  loops' own time  5.63 us (3%)
    psum x1, blocking collectives, per_device(): lax.psum((every_head, query_gain_part, key_gain_part), ('sp', 'tp'))  41.8 us
    reshape x4, local copies, waits for them, and re-layouts, tap_totals(): flattened = jnp.pad(widened.reshape(-1), (0, block))  16.2 us
    ppermute x4, waiting for transfers between devices, shifted(): return lax.ppermute(block, axis, route)  16.1 us
    reshape x4, local copies, waits for them, and re-layouts, bias_matrix(): return flattened.reshape(block, 3 * block - 1)[:, :2 * block]  15.9 us
    pad x4, other arithmetic, tap_totals(): flattened = jnp.pad(widened.reshape(-1), (0, block))  12 us
    reshape x4, local copies, waits for them, and re-layouts, tap_totals(): columns = jnp.sum(flattened.reshape(block, 3 * block), axis=0)  11.3 us
    ppermute x4, starting transfers between devices, shifted(): return lax.ppermute(block, axis, route)  10.9 us
    another operation x8, local copies, waits for them, and re-layouts, bias_matrix(): flattened = jnp.tile(diagonal, block)[:block * (3 * block - 1)]  8.97 us
  transfers between devices with their start and end apart: 4, of which 4 were waited for; matrix products, arithmetic and copies ran while one was open for 2% of the time, Pallas kernels for 0%

commit v1 on v0

v1 whole, which is shorter than its diff:
```python
import functools

import jax
import jax.numpy as jnp
from jax import lax
from jax.experimental import pallas as pl
from jax.experimental.pallas import tpu as pltpu
from jax.sharding import PartitionSpec as P

SEG = 64
PREV = 8
CLIP = 128
LANES = 128
TILE = 128

epsilon = 1e-06
f32 = jnp.float32
bf16 = jnp.bfloat16

ROWS_COLS = (((1,), (1,)), ((), ()))
ROWS_ROWS = (((0,), (0,)), ((), ()))


def shifted(block, axis, distance):
    devices = range(lax.axis_size(axis))
    route = [(i - distance, i) for i in devices if i - distance in devices]
    return lax.ppermute(block, axis, route)


def iota(shape, dim):
    return lax.broadcasted_iota(jnp.int32, shape, dim)


def head_mean(x, head_width):
    same = iota((LANES, LANES), 0) // head_width == iota((LANES, LANES), 1) // head_width
    ones = jnp.where(same, 1.0 / head_width, 0.0).astype(bf16)
    high = x.astype(bf16)
    low = (x - high.astype(f32)).astype(bf16)
    return jnp.dot(high, ones, preferred_element_type=f32) + jnp.dot(
        low, ones, preferred_element_type=f32
    )


def exact_dot(selector, x):
    high = x.astype(bf16)
    low = (x - high.astype(f32)).astype(bf16)
    return jnp.dot(selector, high, preferred_element_type=f32) + jnp.dot(
        selector, low, preferred_element_type=f32
    )


def unit_and_scale(rows, head_width):
    widened = rows.astype(f32)
    scale = lax.rsqrt(head_mean(widened * widened, head_width) + epsilon)
    return widened * scale, scale


def norm_backward(grad_hat, unit, scale, gain, head_width):
    grad_unit = grad_hat * gain
    inner = head_mean(grad_unit * unit, head_width)
    return scale * (grad_unit - unit * inner)


def rows8(x):
    return jnp.sum(x.reshape(x.shape[0] // 8, 8, x.shape[1]), axis=0)


def main_kernel(
    head_width,
    has_before,
    q_ref,
    k_ref,
    v_ref,
    g_ref,
    kr_ref,
    vr_ref,
    q_gain_ref,
    k_gain_ref,
    near_ref,
    dq_ref,
    dk_ref,
    dv_ref,
    dkr_ref,
    dvr_ref,
    stats_ref,
    qs,
    gs,
    kh,
    ku,
    ebuf,
    dbuf,
    pbuf,
    sbuf,
):
    pair = pl.program_id(0)
    rows = q_ref.shape[0]
    tiles = rows // TILE
    wide = 2 * TILE
    score_scale = head_width ** (-0.5)
    before = has_before[0].astype(f32)
    q_gain = q_gain_ref[...]
    k_gain = k_gain_ref[...]

    for part, ref in enumerate((kr_ref, k_ref)):
        unit, _ = unit_and_scale(ref[...], head_width)
        ku[pl.ds(part * rows, rows), :] = unit
        kh[pl.ds(part * rows, rows), :] = (unit * k_gain).astype(bf16)

    lane = iota((TILE, LANES), 1)
    first = lane < head_width
    q_unit, q_scale = unit_and_scale(q_ref[...], head_width)
    q_hat = (q_unit * q_gain).astype(bf16)
    zero = jnp.zeros((TILE, LANES), bf16)
    for b in range(tiles):
        part = q_hat[b * TILE : (b + 1) * TILE, :] * jnp.asarray(score_scale, bf16)
        grad = g_ref[pl.ds(b * TILE, TILE), :]
        qs[pl.ds(b * wide, TILE), :] = jnp.where(first, part, zero)
        qs[pl.ds(b * wide + TILE, TILE), :] = jnp.where(first, zero, part)
        gs[pl.ds(b * wide, TILE), :] = jnp.where(first, grad, zero)
        gs[pl.ds(b * wide + TILE, TILE), :] = jnp.where(first, zero, grad)

    key_pos = iota((TILE, wide), 0)
    query_pos = iota((TILE, wide), 1) % TILE
    causal = query_pos >= key_pos
    inside = key_pos // SEG >= query_pos // SEG
    near = near_ref[pl.ds(2 * pair, 2), :]
    skewed = [
        pltpu.roll(
            jnp.broadcast_to(near[h : h + 1, :], (TILE, TILE)), 0, 1, stride=1, stride_axis=0
        )
        for h in range(2)
    ]
    bias = jnp.concatenate(skewed, axis=1)
    bias_below = jnp.where(causal, 0.0, bias)

    near_grad = jnp.zeros((TILE, wide), f32)
    total = jnp.zeros((1, wide), f32)
    q_gain_grad = jnp.zeros((1, LANES), f32)
    for b in range(tiles):
        q_tile = qs[pl.ds(b * wide, wide), :]
        g_tile = gs[pl.ds(b * wide, wide), :]
        own_sum = jnp.zeros((8, wide), f32)
        before_sum = jnp.zeros((8, wide), f32)
        weighted = jnp.zeros((8, wide), f32)
        for j in range(tiles + 1):
            a = b + j
            scores = lax.dot_general(
                kh[pl.ds(a * TILE, TILE), :], q_tile, ROWS_COLS, preferred_element_type=f32
            )
            if j == tiles:
                scores = scores + bias
            if j == tiles - 1:
                scores = scores + bias_below
            e = jnp.exp(scores)
            if j == tiles:
                e = jnp.where(causal, e, 0.0)
            if j == 0:
                e = jnp.where(inside, e, 0.0)
            v_tile = (
                vr_ref[pl.ds(a * TILE, TILE), :]
                if a < tiles
                else v_ref[pl.ds((a - tiles) * TILE, TILE), :]
            )
            d = lax.dot_general(v_tile, g_tile, ROWS_COLS, preferred_element_type=f32)
            if a < tiles:
                before_sum = before_sum + rows8(e)
            else:
                own_sum = own_sum + rows8(e)
            weighted = weighted + rows8(e * d)
            ebuf[pl.ds(j * TILE, TILE), :] = e
            dbuf[pl.ds(j * TILE, TILE), :] = d
        normalizer = jnp.sum(own_sum + before_sum * before, axis=0, keepdims=True)
        weighted = jnp.sum(weighted, axis=0, keepdims=True)
        inverse = 1.0 / normalizer
        delta = weighted * inverse
        inverse_before = inverse * before
        total = total + (weighted - delta * normalizer) * inverse
        for j in range(tiles + 1):
            a = b + j
            attention = ebuf[pl.ds(j * TILE, TILE), :] * (
                inverse_before if a < tiles else inverse
            )
            score_grad = attention * (dbuf[pl.ds(j * TILE, TILE), :] - delta)
            if j == tiles:
                near_grad = near_grad + score_grad
            if j == tiles - 1:
                near_grad = near_grad + jnp.where(causal, 0.0, score_grad)
            pbuf[pl.ds(a * TILE, TILE), pl.ds(b * wide, wide)] = attention.astype(bf16)
            sbuf[pl.ds(a * TILE, TILE), pl.ds(b * wide, wide)] = score_grad.astype(bf16)
        span = (tiles + 1) * TILE
        turned = lax.dot_general(
            kh[pl.ds(b * TILE, span), :],
            sbuf[pl.ds(b * TILE, span), pl.ds(b * wide, wide)],
            ROWS_ROWS,
            preferred_element_type=f32,
        )
        turned = jnp.concatenate([turned[:head_width, :TILE], turned[head_width:, TILE:]], axis=0)
        grad_hat = turned.T * score_scale
        rows_b = slice(b * TILE, (b + 1) * TILE)
        unit = q_unit[rows_b, :]
        dq_ref[pl.ds(b * TILE, TILE), :] = norm_backward(
            grad_hat, unit, q_scale[rows_b, :], q_gain, head_width
        ).astype(bf16)
        q_gain_grad = q_gain_grad + jnp.sum(grad_hat * unit, axis=0, keepdims=True)

    k_gain_grad = jnp.zeros((1, LANES), f32)
    for a in range(2 * tiles):
        low, high = max(0, a - tiles), min(tiles - 1, a)
        at = pl.ds(low * wide, (high - low + 1) * wide)
        keys = pl.ds(a * TILE, TILE)
        dv = jnp.dot(pbuf[keys, at], gs[at, :], preferred_element_type=f32)
        dk = jnp.dot(sbuf[keys, at], qs[at, :], preferred_element_type=f32)
        k_gain_grad = k_gain_grad + jnp.sum(dk * ku[keys, :], axis=0, keepdims=True)
        if a < tiles:
            dkr_ref[keys, :] = dk.astype(bf16)
            dvr_ref[keys, :] = dv.astype(bf16)
        else:
            own = pl.ds((a - tiles) * TILE, TILE)
            dk_ref[own, :] = dk
            dv_ref[own, :] = dv

    @pl.when(pair == 0)
    def _():
        stats_ref[...] = jnp.zeros_like(stats_ref)

    heads = near_ref.shape[0]
    one_lane = iota((1, LANES), 1)
    flip = iota((TILE, TILE), 0) + iota((TILE, TILE), 1) == TILE - 1
    near_grad = exact_dot(jnp.where(flip, 1.0, 0.0).astype(bf16), near_grad)
    last = jnp.zeros((1, LANES), f32)
    for h in range(2):
        half = slice(h * TILE, (h + 1) * TILE)
        straight = pltpu.roll(near_grad[:, half], 1, 1, stride=1, stride_axis=0)
        taps = jnp.sum(straight, axis=0, keepdims=True)
        stats_ref[pl.ds(2 * pair + h, 1), :] = taps
        rest = jnp.sum(total[:, half] - taps, axis=1, keepdims=True)
        last = last + jnp.where(one_lane == 2 * pair + h, rest, 0.0)
    q_fold = q_gain_grad + pltpu.roll(q_gain_grad, head_width, 1)
    k_fold = k_gain_grad + pltpu.roll(k_gain_grad, head_width, 1)
    stats_ref[pl.ds(heads, 1), :] += jnp.where(one_lane < head_width, q_fold, k_fold)
    stats_ref[pl.ds(heads + 1, 1), :] += last


def final_kernel(
    head_width,
    tp_index,
    k_ref,
    k_gain_ref,
    dk_ref,
    dv_ref,
    dkb_ref,
    dvb_ref,
    all_ref,
    dk_out,
    dv_out,
    q_gain_out,
    k_gain_out,
    bias_out,
):
    unit, scale = unit_and_scale(k_ref[...], head_width)
    grad_hat = dk_ref[...] + dkb_ref[...].astype(f32)
    dk_out[...] = norm_backward(grad_hat, unit, scale, k_gain_ref[...], head_width).astype(bf16)
    dv_out[...] = (dv_ref[...] + dvb_ref[...].astype(f32)).astype(bf16)
    heads = bias_out.shape[0]

    @pl.when(pl.program_id(0) == 0)
    def _():
        everyone = jnp.sum(all_ref[...], axis=0)
        gains = jnp.sum(everyone[:, heads : heads + 1, :], axis=0)
        q_gain_out[...] = gains[:, :head_width]
        k_gain_out[...] = gains[:, head_width:]
        mine = iota(everyone.shape, 0) == tp_index[0]
        summed = jnp.sum(jnp.where(mine, everyone, 0.0), axis=0)
        bias_out[:, :CLIP] = summed[:heads, :]
        row = iota((heads, LANES), 0)
        column = iota((heads, LANES), 1)
        last = jnp.sum(
            jnp.where(row == column, summed[heads + 1 : heads + 2, :], 0.0), axis=1, keepdims=True
        )
        bias_out[:, CLIP:] = last


def per_device(query, key, value, out_grad, query_gain, key_gain, rel_bias):
    rows, width = query.shape
    heads = rel_bias.shape[0]
    head_width = width // heads
    pairs = width // LANES
    copies = LANES // head_width
    before_key = shifted(key, "sp", 1)
    before_value = shifted(value, "sp", 1)
    q_gain = jnp.tile(query_gain[None, :], (1, copies))
    k_gain = jnp.tile(key_gain[None, :], (1, copies))
    near = rel_bias[:, :CLIP] - rel_bias[:, CLIP:]
    has_before = (lax.axis_index("sp") > 0).astype(jnp.int32).reshape(1)
    column = pl.BlockSpec((rows, LANES), lambda p: (0, p))
    whole = lambda shape: pl.BlockSpec(shape, lambda p: (0,) * len(shape))
    stat_rows = -(-(heads + 2) // 8) * 8
    sds = jax.ShapeDtypeStruct
    dq, dk, dv, dk_before, dv_before, stats = pl.pallas_call(
        functools.partial(main_kernel, head_width),
        grid=(pairs,),
        in_specs=[pl.BlockSpec(memory_space=pltpu.SMEM)]
        + [column] * 6
        + [whole((1, LANES)), whole((1, LANES)), whole((heads, CLIP))],
        out_specs=[column] * 5 + [whole((stat_rows, LANES))],
        out_shape=[
            sds((rows, width), bf16),
            sds((rows, width), f32),
            sds((rows, width), f32),
            sds((rows, width), bf16),
            sds((rows, width), bf16),
            sds((stat_rows, LANES), f32),
        ],
        scratch_shapes=[
            pltpu.VMEM((2 * rows, LANES), bf16),
            pltpu.VMEM((2 * rows, LANES), bf16),
            pltpu.VMEM((2 * rows, LANES), bf16),
            pltpu.VMEM((2 * rows, LANES), f32),
            pltpu.VMEM((rows + TILE, 2 * TILE), f32),
            pltpu.VMEM((rows + TILE, 2 * TILE), f32),
            pltpu.VMEM((2 * rows, 2 * rows), bf16),
            pltpu.VMEM((2 * rows, 2 * rows), bf16),
        ],
        name="main",
    )(has_before, query, key, value, out_grad, before_key, before_value, q_gain, k_gain, near)
    dk_back = shifted(dk_before, "sp", -1)
    dv_back = shifted(dv_before, "sp", -1)
    axes = ("sp", "tp")
    members = (lax.axis_size("sp"), lax.axis_size("tp"))
    spread = jnp.broadcast_to(stats[None], (members[0] * members[1],) + stats.shape)
    everyone = lax.all_to_all(spread, axes, 0, 0, tiled=True).reshape(members + stats.shape)
    tp_index = lax.axis_index("tp").astype(jnp.int32).reshape(1)
    dk, dv, q_gain_grad, k_gain_grad, bias_grad = pl.pallas_call(
        functools.partial(final_kernel, head_width),
        grid=(pairs,),
        in_specs=[pl.BlockSpec(memory_space=pltpu.SMEM), column, whole((1, LANES))]
        + [column] * 4
        + [whole(everyone.shape)],
        out_specs=[column, column]
        + [whole((1, head_width)), whole((1, head_width)), whole((heads, CLIP + 1))],
        out_shape=[
            sds((rows, width), bf16),
            sds((rows, width), bf16),
            sds((1, head_width), f32),
            sds((1, head_width), f32),
            sds((heads, CLIP + 1), f32),
        ],
        name="final",
    )(tp_index, key, k_gain, dk, dv, dk_back, dv_back, everyone)
    return (dq, dk, dv, q_gain_grad[0], k_gain_grad[0], bias_grad)


def solution(mesh):
    placed = (P("sp", "tp"), P("sp", "tp"), P("sp", "tp"), P("sp", "tp"), P(), P(), P("tp", None))
    return jax.shard_map(
        per_device,
        mesh=mesh,
        in_specs=placed,
        out_specs=(P("sp", "tp"), P("sp", "tp"), P("sp", "tp"), P(), P(), P("tp", None)),
        check_vma=False,
    )
```

time: 207 us -> 55.1 us (0.27)
  local copies, waits for them, and re-layouts: 72.1 us -> 4.92 us
  blocking collectives: 41.8 us -> 0 us
  matrix products: 35 us -> 0 us
  other arithmetic: 22.7 us -> 0.66 us
  Pallas kernels: 0 us -> 14.8 us
  starting transfers between devices: 10.9 us -> 20.8 us
  loops' own time: 5.63 us -> 0 us
  waiting for transfers between devices: 16.1 us -> 12.8 us
    reshape x12 -> x0, local copies, waits for them, and re-layouts: 43.3 us -> none  [the longest x4 16.2 us: tap_totals(): flattened = jnp.pad(widened.reshape(-1), (0, block))]
    psum x1 -> x0, blocking collectives: 41.8 us -> none  [per_device(): lax.psum((every_head, query_gain_part, key_gain_part), ('sp', 'tp'))]
    dot_general x24 -> x0, matrix products: 35 us -> none  [the longest x4 8.53 us: block_gradients(): jnp.dot(query_block, key_block.T, preferred_element_type=jnp.float32)]
    pallas_call x0 -> x2, Pallas kernels: none -> 14.8 us  [the longest x1 11.6 us: per_device(): pl.pallas_call(functools.partial(main_kernel, head_width), grid=(pairs,),...]
    pad x4 -> x0, other arithmetic: 12 us -> none  [tap_totals(): flattened = jnp.pad(widened.reshape(-1), (0, block))]
    ppermute x4, waiting for transfers between devices: 16.1 us -> 4.64 us  [shifted(): return lax.ppermute(block, axis, route)]
    all_to_all x0 -> x1, starting transfers between devices: none -> 9.87 us  [per_device(): lax.all_to_all(spread, axes, 0, 0, tiled=True)]
    pad x4 -> x0, local copies, waits for them, and re-layouts: 8.21 us -> none  [tap_totals(): widened = jnp.pad(score_grad, ((0, 0), (0, block - 1)))]
  transfers between devices with their start and end apart: 4 -> 5, of which waited for: 4 -> 3; matrix products, arithmetic and copies ran while one was open for 2% -> 6% of each run, Pallas kernels for 0% -> 0%
where the time goes in v1:
time: 55.1 us; the launch traced here: 54.8 us
  starting transfers between devices  20.8 us (38%)
  Pallas kernels  14.8 us (27%)
  waiting for transfers between devices  12.8 us (23%)
  local copies, waits for them, and re-layouts  4.92 us (9%)
  between operations  0.73 us (1%)
  other arithmetic  0.66 us (1%)
    pallas_call x1, Pallas kernels, per_device(): pl.pallas_call(functools.partial(main_kernel, head_width), grid=(pairs,),...  11.6 us
    ppermute x4, starting transfers between devices, shifted(): return lax.ppermute(block, axis, route)  10.9 us
    all_to_all x1, starting transfers between devices, per_device(): lax.all_to_all(spread, axes, 0, 0, tiled=True)  9.87 us
    all_to_all x1, waiting for transfers between devices, per_device(): lax.all_to_all(spread, axes, 0, 0, tiled=True)  8.2 us
    ppermute x4, waiting for transfers between devices, shifted(): return lax.ppermute(block, axis, route)  4.64 us
    pallas_call x1, Pallas kernels, per_device(): pl.pallas_call(functools.partial(final_kernel, head_width), grid=(pairs,)...  3.16 us
    unnamed x18, local copies, waits for them, and re-layouts  2.2 us
  transfers between devices with their start and end apart: 5, of which 3 were waited for; matrix products, arithmetic and copies ran while one was open for 6% of the time, Pallas kernels for 0%

profile of v1, /device:TPU:0, one launch (start us, length us, event | category | flops | bytes accessed | tf_op | source)
XLA Modules:
  0.0 54.8 jit_solution(14467408718715498228)
XLA Ops:
  0.6 4.9 %collective-permute-start.1 = (bf16[512,256]{1,0:T(8,128)(2,1)}, bf16[512,256]{1,0:T(8,128)(2,1)S(1)}, u32[]{:S(2)}, u32[]{:S(2)}) collective-permute-start(bf16[512,256]{1,0:T(8,128)(2,1)} %v_ref.1), channel_id=1, source_target_pairs={{0,4},{4,8},{8,12},{12,16},{16,20},{20,24},{24,28},{1,5},{5,9},{9,... | collective-permute-start | bytes 786440 | tf_op jit(solution)/shard_map/ppermute | solution.py:27
  5.6 3.4 %collective-permute-start = (bf16[512,256]{1,0:T(8,128)(2,1)}, bf16[512,256]{1,0:T(8,128)(2,1)S(1)}, u32[]{:S(2)}, u32[]{:S(2)}) collective-permute-start(bf16[512,256]{1,0:T(8,128)(2,1)} %k_ref.3), channel_id=1, source_target_pairs={{0,4},{4,8},{8,12},{12,16},{16,20},{20,24},{24,28},{1,5},{5,9},{9,... | collective-permute-start | bytes 786440 | tf_op jit(solution)/shard_map/ppermute | solution.py:27
  9.0 0.8 %slice_reduce_fusion = f32[4]{0:T(128)S(1)} fusion(f32[4,129]{1,0:T(4,128)} %param.13), kind=kLoop, calls=%fused_computation | loop fusion | bytes 32 | tf_op jit(solution)/shard_map/slice | solution.py:293
  9.8 0.0 copy-start.7
  9.8 0.0 copy-start.8
  9.8 0.6 %copy-done.7 = f32[64]{0:T(128)S(1)} copy-done((f32[64]{0:T(128)S(1)}, f32[64]{0:T(128)}, u32[]{:S(2)}) %copy-start.7) | copy-done | bytes 280
  10.5 0.0 copy-start.6
  10.5 0.6 %tile.17.q_gain_ref = f32[1,128]{1,0:T(1,128)} reshape(f32[2,64]{1,0:T(2,128)S(1)} %tile.16) | data formatting | bytes 1024 | tf_op jit(solution)/shard_map/tile | solution.py:291
  11.0 0.0 copy-done.8
  11.1 0.7 %tile.19.k_gain_ref = f32[1,128]{1,0:T(1,128)} reshape(f32[2,64]{1,0:T(2,128)S(1)} %tile.18) | data formatting | bytes 1024 | tf_op jit(solution)/shard_map/tile | solution.py:292
  11.7 0.0 copy-done.6
  11.7 0.7 %slice_subtract_fusion.near_ref = f32[4,128]{1,0:T(4,128)} fusion(f32[4,129]{1,0:T(4,128)S(1)} %copy-done.6, f32[4]{0:T(128)S(1)} %slice_reduce_fusion), kind=kLoop, calls=%fused_computation.1 | loop fusion | flops 512 | bytes 4112 | tf_op jit(solution)/shard_map/sub | solution.py:293
  12.4 0.2 collective-permute-done.1.vr_ref
  12.5 0.0 copy-start.1
  12.5 4.5 %collective-permute-done.kr_ref = bf16[512,256]{1,0:T(8,128)(2,1)S(1)} collective-permute-done((bf16[512,256]{1,0:T(8,128)(2,1)}, bf16[512,256]{1,0:T(8,128)(2,1)S(1)}, u32[]{:S(2)}, u32[]{:S(2)}) %collective-permute-start) | collective-permute-done | bytes 262176 | tf_op jit(solution)/shard_map/ppermute | solution.py:27
  17.0 0.0 copy-start.3
  17.0 0.0 copy-done.1
  17.0 0.7 %copy-done.3 = bf16[512,256]{1,0:T(8,128)(2,1)} copy-done((bf16[512,256]{1,0:T(8,128)(2,1)}, bf16[512,256]{1,0:T(8,128)(2,1)S(1)}, u32[]{:S(2)}) %copy-start.3) | copy-done | bytes 262168
  17.7 11.6 %main.1 = (bf16[512,256]{1,0:T(8,128)(2,1)}, f32[512,256]{1,0:T(8,128)}, f32[512,256]{1,0:T(8,128)}, bf16[512,256]{1,0:T(8,128)(2,1)}, bf16[512,256]{1,0:T(8,128)(2,1)}, /*index=5*/f32[8,128]{1,0:T(8,128)}) custom-call(s32[1]{0:T(128)} %bitcast.has_before, bf16[512,256]{1,0:T(8,128)(2,1)} %q_ref.1, bf16[512,256]{1,0:T(8,128)(2,1)} %k_ref.3, ...), custom_call_target="tpu_custom_call" | custom-call | tf_op jit(solution)/shard_map/main/pallas_call | solution.py:299
  29.4 0.0 copy-start.5
  29.4 1.3 %collective-permute-start.2 = (bf16[512,256]{1,0:T(8,128)(2,1)}, bf16[512,256]{1,0:T(8,128)(2,1)S(1)}, u32[]{:S(2)}, u32[]{:S(2)}) collective-permute-start(bf16[512,256]{1,0:T(8,128)(2,1)} %get-tuple-element.20), channel_id=1, source_target_pairs={{4,0},{8,4},{12,8},{16,12},{20,16},{24,20},{28,24},{5,1},{9,5},{13... | collective-permute-start | bytes 786440 | tf_op jit(solution)/shard_map/ppermute | solution.py:27
  30.7 1.3 %collective-permute-start.3 = (bf16[512,256]{1,0:T(8,128)(2,1)}, bf16[512,256]{1,0:T(8,128)(2,1)S(1)}, u32[]{:S(2)}, u32[]{:S(2)}) collective-permute-start(bf16[512,256]{1,0:T(8,128)(2,1)} %get-tuple-element.21), channel_id=1, source_target_pairs={{4,0},{8,4},{12,8},{16,12},{20,16},{24,20},{28,24},{5,1},{9,5},{13... | collective-permute-start | bytes 786440 | tf_op jit(solution)/shard_map/ppermute | solution.py:27
  32.0 0.0 copy-done.5
  32.0 0.7 %broadcast_in_dim.2 = f32[32,8,128]{2,1,0:T(8,128)} broadcast(f32[8,128]{1,0:T(8,128)S(1)} %copy-done.5), dimensions={1,2} | broadcast | bytes 135168 | tf_op jit(solution)/shard_map/broadcast_in_dim | solution.py:330
  32.7 9.9 %all-to-all-start = ((f32[32,8,128]{2,1,0:T(8,128)}), f32[32,8,128]{2,1,0:T(8,128)S(1)}, u32[]{:S(2)}, u32[]{:S(2)}) async-start(f32[32,8,128]{2,1,0:T(8,128)} %broadcast_in_dim.2), calls=%async_computation | async-start | bytes 262144 | tf_op jit(solution)/shard_map/all_to_all | solution.py:331
  42.5 8.2 %all-to-all-done = f32[32,8,128]{2,1,0:T(8,128)S(1)} async-done(((f32[32,8,128]{2,1,0:T(8,128)}), f32[32,8,128]{2,1,0:T(8,128)S(1)}, u32[]{:S(2)}, u32[]{:S(2)}) %all-to-all-start) | async-done | bytes 131104 | tf_op jit(solution)/shard_map/all_to_all | solution.py:331
  50.7 0.0 copy-start
  50.7 0.0 collective-permute-done.2.dkb_ref
  50.7 0.0 copy-start.2
  50.7 0.0 collective-permute-done.3.dvb_ref
  50.8 0.0 copy-start.4
  50.8 0.6 %copy-done = f32[32,8,128]{2,1,0:T(8,128)} copy-done((f32[32,8,128]{2,1,0:T(8,128)}, f32[32,8,128]{2,1,0:T(8,128)S(1)}, u32[]{:S(2)}) %copy-start) | copy-done | bytes 131096
  51.4 0.1 copy-done.2
  51.5 0.1 copy-done.4
  51.6 3.2 %final.1 = (bf16[512,256]{1,0:T(8,128)(2,1)}, bf16[512,256]{1,0:T(8,128)(2,1)}, f32[1,64]{1,0:T(1,128)}, f32[1,64]{1,0:T(1,128)}, f32[4,129]{1,0:T(4,128)}) custom-call(s32[1]{0:T(128)} %bitcast.1.tp_index, bf16[512,256]{1,0:T(8,128)(2,1)} %k_ref.3, f32[1,128]{1,0:T(1,128)} %tile.19.k_gain_ref, f32[512,256]{1,0:T(8,128)} %get-tuple-element.18.dk_ref, ...), custom_call_target="tpu_custom_call" | custom-call | tf_op jit(solution)/shard_map/final/pallas_call | solution.py:333
  (2 shorter events, 0.0 us)
Async XLA Ops:
  0.6 11.9 %collective-permute-start.1 = (bf16[512,256]{1,0:T(8,128)(2,1)}, bf16[512,256]{1,0:T(8,128)(2,1)S(1)}, u32[]{:S(2)}, u32[]{:S(2)}) collective-permute-start(bf16[512,256]{1,0:T(8,128)(2,1)} %v_ref.1), channel_id=1, source_target_pairs={{0,4},{4,8},{8,12},{12,16},{16,20},{20,24},{24,28},{1,5},{5,9},{9,... | collective-permute-start | bytes 786440 | tf_op jit(solution)/shard_map/ppermute | solution.py:27
  5.6 11.5 %collective-permute-start = (bf16[512,256]{1,0:T(8,128)(2,1)}, bf16[512,256]{1,0:T(8,128)(2,1)S(1)}, u32[]{:S(2)}, u32[]{:S(2)}) collective-permute-start(bf16[512,256]{1,0:T(8,128)(2,1)} %k_ref.3), channel_id=1, source_target_pairs={{0,4},{4,8},{8,12},{12,16},{16,20},{20,24},{24,28},{1,5},{5,9},{9,... | collective-permute-start | bytes 786440 | tf_op jit(solution)/shard_map/ppermute | solution.py:27
  9.8 0.7 %copy-start.7 = (f32[64]{0:T(128)S(1)}, f32[64]{0:T(128)}, u32[]{:S(2)}) copy-start(f32[64]{0:T(128)} %param.11) | copy-start | bytes 772
  9.8 1.2 %copy-start.8 = (f32[64]{0:T(128)S(1)}, f32[64]{0:T(128)}, u32[]{:S(2)}) copy-start(f32[64]{0:T(128)} %param.12) | copy-start | bytes 772
  10.5 1.3 %copy-start.6 = (f32[4,129]{1,0:T(4,128)S(1)}, f32[4,129]{1,0:T(4,128)}, u32[]{:S(2)}) copy-start(f32[4,129]{1,0:T(4,128)} %param.13) | copy-start | bytes 6196
  12.5 4.5 %copy-start.1 = (bf16[512,256]{1,0:T(8,128)(2,1)}, bf16[512,256]{1,0:T(8,128)(2,1)S(1)}, u32[]{:S(2)}) copy-start(bf16[512,256]{1,0:T(8,128)(2,1)S(1)} %collective-permute-done.1.vr_ref) | copy-start | bytes 786436
  17.0 0.7 %copy-start.3 = (bf16[512,256]{1,0:T(8,128)(2,1)}, bf16[512,256]{1,0:T(8,128)(2,1)S(1)}, u32[]{:S(2)}) copy-start(bf16[512,256]{1,0:T(8,128)(2,1)S(1)} %collective-permute-done.kr_ref) | copy-start | bytes 786436
  29.4 2.6 %copy-start.5 = (f32[8,128]{1,0:T(8,128)S(1)}, f32[8,128]{1,0:T(8,128)}, u32[]{:S(2)}) copy-start(f32[8,128]{1,0:T(8,128)} %get-tuple-element.22) | copy-start | bytes 12292
  29.4 21.4 %collective-permute-start.2 = (bf16[512,256]{1,0:T(8,128)(2,1)}, bf16[512,256]{1,0:T(8,128)(2,1)S(1)}, u32[]{:S(2)}, u32[]{:S(2)}) collective-permute-start(bf16[512,256]{1,0:T(8,128)(2,1)} %get-tuple-element.20), channel_id=1, source_target_pairs={{4,0},{8,4},{12,8},{16,12},{20,16},{24,20},{28,24},{5,1},{9,5},{13... | collective-permute-start | bytes 786440 | tf_op jit(solution)/shard_map/ppermute | solution.py:27
  30.7 20.1 %collective-permute-start.3 = (bf16[512,256]{1,0:T(8,128)(2,1)}, bf16[512,256]{1,0:T(8,128)(2,1)S(1)}, u32[]{:S(2)}, u32[]{:S(2)}) collective-permute-start(bf16[512,256]{1,0:T(8,128)(2,1)} %get-tuple-element.21), channel_id=1, source_target_pairs={{4,0},{8,4},{12,8},{16,12},{20,16},{24,20},{28,24},{5,1},{9,5},{13... | collective-permute-start | bytes 786440 | tf_op jit(solution)/shard_map/ppermute | solution.py:27
  32.7 18.1 %all-to-all-start = ((f32[32,8,128]{2,1,0:T(8,128)}), f32[32,8,128]{2,1,0:T(8,128)S(1)}, u32[]{:S(2)}, u32[]{:S(2)}) async-start(f32[32,8,128]{2,1,0:T(8,128)} %broadcast_in_dim.2), calls=%async_computation | async-start | bytes 262144 | tf_op jit(solution)/shard_map/all_to_all | solution.py:331
  50.7 0.6 %copy-start = (f32[32,8,128]{2,1,0:T(8,128)}, f32[32,8,128]{2,1,0:T(8,128)S(1)}, u32[]{:S(2)}) copy-start(f32[32,8,128]{2,1,0:T(8,128)S(1)} %all-to-all-done) | copy-start | bytes 393220
  50.7 0.8 %copy-start.2 = (bf16[512,256]{1,0:T(8,128)(2,1)}, bf16[512,256]{1,0:T(8,128)(2,1)S(1)}, u32[]{:S(2)}) copy-start(bf16[512,256]{1,0:T(8,128)(2,1)S(1)} %collective-permute-done.2.dkb_ref) | copy-start | bytes 786436
  50.8 0.9 %copy-start.4 = (bf16[512,256]{1,0:T(8,128)(2,1)}, bf16[512,256]{1,0:T(8,128)(2,1)S(1)}, u32[]{:S(2)}) copy-start(bf16[512,256]{1,0:T(8,128)(2,1)S(1)} %collective-permute-done.3.dvb_ref) | copy-start | bytes 786436

commit v2 on v0

v2 whole, which is shorter than its diff:
```python
import jax
import jax.numpy as jnp
from jax import lax
from jax.experimental import pallas as pl
from jax.experimental.pallas import tpu as pltpu
from jax.sharding import PartitionSpec as P


SEG = 64
CLIP = 128
LANES = 128
TILE = 128
WIDE = 2 * TILE
GRANT = 12 * 1024 * 1024

epsilon = 1e-06
f32 = jnp.float32
bf16 = jnp.bfloat16

ROWS_COLS = (((1,), (1,)), ((), ()))


def shifted(block, axis, distance):
    devices = range(lax.axis_size(axis))
    route = [(i - distance, i) for i in devices if i - distance in devices]
    return lax.ppermute(block, axis, route)


def iota(shape, dim):
    return lax.broadcasted_iota(jnp.int32, shape, dim)


def split_dot(x, matrix):
    high = x.astype(bf16)
    low = (x - high.astype(f32)).astype(bf16)
    return jnp.dot(high, matrix, preferred_element_type=f32) + jnp.dot(
        low, matrix, preferred_element_type=f32
    )


def head_mean(x, head_width):
    same = iota((LANES, LANES), 0) // head_width == iota((LANES, LANES), 1) // head_width
    return split_dot(x, jnp.where(same, 1.0 / head_width, 0.0).astype(bf16))


def unit_and_scale(rows, head_width):
    widened = rows.astype(f32)
    scale = lax.rsqrt(head_mean(widened * widened, head_width) + epsilon)
    return widened * scale, scale


def norm_backward(grad_hat, unit, scale, gain, head_width):
    grad_unit = grad_hat * gain
    inner = head_mean(grad_unit * unit, head_width)
    return scale * (grad_unit - unit * inner)


def rows8(x):
    return jnp.sum(x.reshape(x.shape[0] // 8, 8, x.shape[1]), axis=0)


def both_heads(gain_ref):
    gain = gain_ref[...]
    return jnp.concatenate([gain] * (LANES // gain.shape[1]), axis=1)


def each_pair(pairs, body):
    for p in range(pairs):
        body(p)


def at(tile):
    return pl.ds(tile * TILE, TILE)


def masks():
    key_pos = iota((TILE, WIDE), 0)
    query_pos = iota((TILE, WIDE), 1) % TILE
    return query_pos >= key_pos, key_pos // SEG >= query_pos // SEG


def as_column(row, rows):
    turned = jnp.broadcast_to(row, (LANES, rows)).T
    return turned


def own_kernel(
    q_hbm, k_hbm, v_hbm, g_hbm, q_gain_hbm, k_gain_hbm, table_hbm,
    qs_ref, gs_ref, kt_ref, ku_ref, qu_ref, qscale_ref, e_ref, sum_ref, weighted_ref, bias_ref,
    gains_ref, kh_ref, q_ref, k_ref, v_ref, g_ref, q_gain_ref, k_gain_ref, table_ref, sems,
):
    sources = (q_gain_hbm, k_gain_hbm, table_hbm, k_hbm, q_hbm, g_hbm, v_hbm)
    targets = (q_gain_ref, k_gain_ref, table_ref, k_ref, q_ref, g_ref, v_ref)
    copies = [
        pltpu.make_async_copy(source, target, sems.at[i])
        for i, (source, target) in enumerate(zip(sources, targets))
    ]
    for copy in copies:
        copy.start()
    for copy in copies:
        copy.wait()
    rows = q_ref.shape[0]
    tiles = rows // TILE
    head_width = q_gain_ref.shape[1]
    q_gain, k_gain = both_heads(q_gain_ref), both_heads(k_gain_ref)
    gains_ref[...] = jnp.concatenate([q_gain, k_gain, jnp.zeros((6, LANES), f32)], axis=0)
    causal, _ = masks()
    first = iota((TILE, LANES), 1) < head_width
    zero = jnp.zeros((TILE, LANES), bf16)
    table = table_ref[...]
    near = table[:, :CLIP] - table[:, CLIP:]

    def body(p):
        lanes = pl.ds(p * LANES, LANES)
        unit, _ = unit_and_scale(k_ref[:, lanes], head_width)
        ku_ref[p] = unit
        hat = (unit * k_gain).astype(bf16)
        kh_ref[p] = hat
        kt_ref[p] = hat.T
        unit, scale = unit_and_scale(q_ref[:, lanes], head_width)
        qu_ref[p] = unit
        qscale_ref[p] = scale
        hat = (unit * q_gain).astype(bf16) * jnp.asarray(head_width ** (-0.5), bf16)
        for b in range(tiles):
            part = hat[b * TILE : (b + 1) * TILE, :]
            grad = g_ref[at(b), lanes]
            qs_ref[p, pl.ds(b * WIDE, TILE), :] = jnp.where(first, part, zero)
            qs_ref[p, pl.ds(b * WIDE + TILE, TILE), :] = jnp.where(first, zero, part)
            gs_ref[p, pl.ds(b * WIDE, TILE), :] = jnp.where(first, grad, zero)
            gs_ref[p, pl.ds(b * WIDE + TILE, TILE), :] = jnp.where(first, zero, grad)
        skewed = [
            pltpu.roll(
                jnp.broadcast_to(near[2 * p + h : 2 * p + h + 1, :], (TILE, TILE)),
                0,
                1,
                stride=1,
                stride_axis=0,
            )
            for h in range(2)
        ]
        bias = jnp.concatenate(skewed, axis=1)
        below = jnp.where(causal, 0.0, bias)
        bias_ref[p] = below
        for b in range(tiles):
            queries = pl.ds(b * WIDE, WIDE)
            q_tile, g_tile = qs_ref[p, queries, :], gs_ref[p, queries, :]
            total = jnp.zeros((8, WIDE), f32)
            weighted = jnp.zeros((8, WIDE), f32)
            for a in range(b + 1):
                scores = lax.dot_general(
                    kh_ref[p, at(a), :], q_tile, ROWS_COLS, preferred_element_type=f32
                )
                if a == b:
                    scores = scores + bias
                if a == b - 1:
                    scores = scores + below
                e = jnp.exp(scores)
                if a == b:
                    e = jnp.where(causal, e, 0.0)
                d = lax.dot_general(
                    v_ref[at(a), lanes], g_tile, ROWS_COLS, preferred_element_type=f32
                )
                total = total + rows8(e)
                weighted = weighted + rows8(e * d)
                e_ref[p, at(a), queries] = e.astype(bf16)
            sum_ref[p, :, queries] = total
            weighted_ref[p, :, queries] = weighted

    each_pair(qs_ref.shape[0], body)


def before_kernel(
    has_before, kr_ref, gains_ref, qs_ref, gs_ref, e_ref, sum_ref, bias_ref,
    krt_ref, kru_ref, er_ref, norm_ref, qn_ref, dv_ref, dvr_ref, krh_ref, gn_ref,
):
    rows, width = kr_ref.shape
    tiles = rows // TILE
    head_width = width // (2 * qs_ref.shape[0])
    before = has_before[0].astype(f32)
    k_gain = gains_ref[1:2, :]
    _, inside = masks()

    def body(p):
        lanes = pl.ds(p * LANES, LANES)
        unit, _ = unit_and_scale(kr_ref[:, lanes], head_width)
        kru_ref[p] = unit
        hat = (unit * k_gain).astype(bf16)
        krh_ref[p] = hat
        krt_ref[p] = hat.T
        for b in range(tiles):
            queries = pl.ds(b * WIDE, WIDE)
            q_tile = qs_ref[p, queries, :]
            total = jnp.zeros((8, WIDE), f32)
            for a in range(b, tiles):
                scores = lax.dot_general(
                    krh_ref[p, at(a), :], q_tile, ROWS_COLS, preferred_element_type=f32
                )
                if b == 0 and a == tiles - 1:
                    scores = scores + bias_ref[p]
                e = jnp.exp(scores)
                if a == b:
                    e = jnp.where(inside, e, 0.0)
                total = total + rows8(e)
                er_ref[p, at(a), queries] = e.astype(bf16)
            normalizer = jnp.sum(
                sum_ref[p, :, queries] + total * before, axis=0, keepdims=True
            )
            norm_ref[p, :, queries] = jnp.broadcast_to(normalizer, (8, WIDE))
            column = as_column(1.0 / normalizer, WIDE)
            qn_ref[p, queries, :] = (q_tile.astype(f32) * column).astype(bf16)
            gn_ref[queries, :] = (gs_ref[p, queries, :].astype(f32) * column).astype(bf16)
        for a in range(tiles):
            span = pl.ds(0, (a + 1) * WIDE)
            dvr_ref[at(a), lanes] = jnp.dot(
                er_ref[p, at(a), span], gn_ref[span, :], preferred_element_type=f32
            ).astype(bf16)
        for a in range(tiles):
            span = pl.ds(a * WIDE, (tiles - a) * WIDE)
            dv_ref[at(a), lanes] = jnp.dot(
                e_ref[p, at(a), span], gn_ref[span, :], preferred_element_type=f32
            )

    each_pair(qs_ref.shape[0], body)


def grad_kernel(
    has_before, vr_ref, v_ref, gs_ref, qn_ref, kt_ref, krt_ref, ku_ref, kru_ref, qu_ref,
    qscale_ref, e_ref, er_ref, norm_ref, weighted_ref, gains_ref,
    dq_ref, dk_ref, dkr_ref, stats_ref, s_ref, sr_ref, delta_ref, turned_ref,
):
    rows, width = v_ref.shape
    tiles = rows // TILE
    pairs = qn_ref.shape[0]
    heads = 2 * pairs
    head_width = width // heads
    before = has_before[0].astype(f32)
    q_gain = gains_ref[0:1, :]
    causal, _ = masks()
    one_lane = iota((1, LANES), 1)
    flip = iota((TILE, TILE), 0) + iota((TILE, TILE), 1) == TILE - 1
    flip = jnp.where(flip, 1.0, 0.0).astype(bf16)

    for p in range(pairs):
        lanes = pl.ds(p * LANES, LANES)
        for b in range(tiles):
            queries = pl.ds(b * WIDE, WIDE)
            g_tile = gs_ref[p, queries, :]
            weighted = weighted_ref[p, :, queries]
            for a in range(b, tiles):
                d = lax.dot_general(
                    vr_ref[at(a), lanes], g_tile, ROWS_COLS, preferred_element_type=f32
                )
                weighted = weighted + rows8(er_ref[p, at(a), queries].astype(f32) * d)
            weighted = jnp.sum(weighted, axis=0, keepdims=True)
            normalizer = norm_ref[p, 0:1, queries]
            inverse = 1.0 / normalizer
            delta = weighted * inverse
            rest = (weighted - delta * normalizer) * inverse
            delta_ref[p, :, queries] = jnp.concatenate([inverse, delta, rest], axis=0)
    for p in range(pairs):
        lanes = pl.ds(p * LANES, LANES)
        for b in range(tiles):
            queries = pl.ds(b * WIDE, WIDE)
            g_tile = gs_ref[p, queries, :]
            delta = delta_ref[p, 1:2, queries]
            for a in range(b, tiles):
                d = lax.dot_general(
                    vr_ref[at(a), lanes], g_tile, ROWS_COLS, preferred_element_type=f32
                )
                s = er_ref[p, at(a), queries].astype(f32) * (d - delta)
                sr_ref[p, at(a), queries] = s.astype(bf16)
            for a in range(b + 1):
                d = lax.dot_general(
                    v_ref[at(a), lanes], g_tile, ROWS_COLS, preferred_element_type=f32
                )
                s = e_ref[p, at(a), queries].astype(f32) * (d - delta)
                s_ref[p, at(a), queries] = s.astype(bf16)
    for p in range(pairs):
        for b in range(tiles):
            queries = pl.ds(b * WIDE, WIDE)
            own, old = pl.ds(0, (b + 1) * TILE), pl.ds(b * TILE, (tiles - b) * TILE)
            turned = jnp.dot(
                kt_ref[p, :, own], s_ref[p, own, queries], preferred_element_type=f32
            ) + jnp.dot(
                krt_ref[p, :, old], sr_ref[p, old, queries], preferred_element_type=f32
            )
            turned = turned * (delta_ref[p, 0:1, queries] * head_width ** (-0.5))
            turned = jnp.concatenate(
                [turned[:head_width, :TILE], turned[head_width:, TILE:]], axis=0
            )
            turned_ref[p, at(b), :] = turned.T
    k_sum = jnp.zeros((1, LANES), f32)
    q_sum = jnp.zeros((1, LANES), f32)
    for p in range(pairs):
        lanes = pl.ds(p * LANES, LANES)
        for a in range(tiles):
            span = pl.ds(0, (a + 1) * WIDE)
            dk = jnp.dot(sr_ref[p, at(a), span], qn_ref[p, span, :], preferred_element_type=f32)
            k_sum = k_sum + jnp.sum(dk * kru_ref[p, at(a), :], axis=0, keepdims=True)
            dkr_ref[at(a), lanes] = dk.astype(bf16)
        for a in range(tiles):
            span = pl.ds(a * WIDE, (tiles - a) * WIDE)
            dk = jnp.dot(s_ref[p, at(a), span], qn_ref[p, span, :], preferred_element_type=f32)
            k_sum = k_sum + jnp.sum(dk * ku_ref[p, at(a), :], axis=0, keepdims=True)
            dk_ref[at(a), lanes] = dk
    lines = []
    last = jnp.zeros((1, LANES), f32)
    for p in range(pairs):
        lanes = pl.ds(p * LANES, LANES)
        grad_hat = turned_ref[p]
        unit = qu_ref[p]
        dq_ref[:, lanes] = norm_backward(
            grad_hat, unit, qscale_ref[p], q_gain, head_width
        ).astype(bf16)
        q_sum = q_sum + jnp.sum(grad_hat * unit, axis=0, keepdims=True)
        near_grad = jnp.zeros((TILE, WIDE), f32)
        total = jnp.zeros((1, WIDE), f32)
        for b in range(tiles):
            queries = pl.ds(b * WIDE, WIDE)
            inverse = delta_ref[p, 0:1, queries]
            total = total + delta_ref[p, 2:3, queries]
            below = s_ref[p, at(b - 1), queries] if b else sr_ref[p, at(tiles - 1), queries]
            below = below.astype(f32) * (inverse if b else inverse * before)
            exact = s_ref[p, at(b), queries].astype(f32) * inverse
            near_grad = near_grad + jnp.where(causal, exact, below)
        near_grad = split_dot_left(flip, near_grad)
        for h in range(2):
            half = slice(h * TILE, (h + 1) * TILE)
            straight = pltpu.roll(near_grad[:, half], 1, 1, stride=1, stride_axis=0)
            taps = jnp.sum(straight, axis=0, keepdims=True)
            lines.append(taps)
            rest = jnp.sum(total[:, half] - taps, axis=1, keepdims=True)
            last = last + jnp.where(one_lane == 2 * p + h, rest, 0.0)
    q_fold = q_sum + pltpu.roll(q_sum, head_width, 1)
    k_fold = k_sum + pltpu.roll(k_sum, head_width, 1)
    lines.append(jnp.where(one_lane < head_width, q_fold, k_fold))
    lines.append(last)
    lines.append(jnp.zeros((stats_ref.shape[1] - len(lines), LANES), f32))
    stats_ref[...] = jnp.broadcast_to(jnp.concatenate(lines, axis=0)[None], stats_ref.shape)


def split_dot_left(matrix, x):
    high = x.astype(bf16)
    low = (x - high.astype(f32)).astype(bf16)
    return jnp.dot(matrix, high, preferred_element_type=f32) + jnp.dot(
        matrix, low, preferred_element_type=f32
    )


def final_kernel(
    tp_index, gains_ref, k_ref, dk_ref, dv_ref, dkb_ref, dvb_ref, all_ref,
    dk_out, dv_out, q_gain_out, k_gain_out, bias_out,
):
    _, width = dk_ref.shape
    head_width = width // bias_out.shape[0]
    k_gain = gains_ref[1:2, :]

    def body(p):
        lanes = pl.ds(p * LANES, LANES)
        unit, scale = unit_and_scale(k_ref[:, lanes], head_width)
        grad_hat = dk_ref[:, lanes] + dkb_ref[:, lanes].astype(f32)
        dk_out[:, lanes] = norm_backward(grad_hat, unit, scale, k_gain, head_width).astype(bf16)
        dv_out[:, lanes] = (dv_ref[:, lanes] + dvb_ref[:, lanes].astype(f32)).astype(bf16)

    each_pair(width // LANES, body)
    heads = bias_out.shape[0]
    everyone = jnp.sum(all_ref[...], axis=0)
    gains = jnp.sum(everyone[:, heads : heads + 1, :], axis=0)
    q_gain_out[...] = gains[:, :head_width]
    k_gain_out[...] = gains[:, head_width:]
    mine = iota(everyone.shape, 0) == tp_index[0]
    summed = jnp.sum(jnp.where(mine, everyone, 0.0), axis=0)
    bias_out[:, :CLIP] = summed[:heads, :]
    diagonal = iota((heads, LANES), 0) == iota((heads, LANES), 1)
    last = jnp.where(diagonal, summed[heads + 1 : heads + 2, :], 0.0)
    bias_out[:, CLIP:] = jnp.sum(last, axis=1, keepdims=True)


def call(kernel, args, outs, scratch=(), scalars=0, hbm=0, flops=0):
    args = [
        pltpu.with_memory_space_constraint(x, pltpu.HBM) if scalars <= i < scalars + hbm else x
        for i, x in enumerate(args)
    ]
    specs = [pl.BlockSpec(memory_space=pltpu.SMEM)] * scalars
    specs += [pl.BlockSpec(memory_space=pltpu.HBM)] * hbm
    specs += [pl.BlockSpec(memory_space=pltpu.VMEM)] * (len(args) - scalars - hbm)
    return pl.pallas_call(
        kernel,
        in_specs=specs,
        out_specs=[pl.BlockSpec(memory_space=pltpu.VMEM)] * len(outs),
        out_shape=[jax.ShapeDtypeStruct(*o) for o in outs],
        scratch_shapes=list(scratch),
        compiler_params=pltpu.CompilerParams(vmem_limit_bytes=GRANT),
        cost_estimate=pl.CostEstimate(flops=flops, bytes_accessed=0, transcendentals=0),
    )(*args)


def per_device(query, key, value, out_grad, query_gain, key_gain, rel_bias):
    rows, width = query.shape
    heads = rel_bias.shape[0]
    head_width = width // heads
    pairs = width // LANES
    double = 2 * rows
    before_key = shifted(key, "sp", 1)
    before_value = shifted(value, "sp", 1)
    q_gain, k_gain = query_gain[None, :], key_gain[None, :]
    has_before = (lax.axis_index("sp") > 0).astype(jnp.int32).reshape(1)
    tp_index = lax.axis_index("tp").astype(jnp.int32).reshape(1)
    stacked = ((pairs, double, LANES), bf16)
    hats = ((pairs, rows, LANES), bf16)
    turned = ((pairs, LANES, rows), bf16)
    units = ((pairs, rows, LANES), f32)
    square = ((pairs, rows, double), bf16)
    line = ((pairs, 8, double), f32)
    flat, flat_low = ((rows, width), f32), ((rows, width), bf16)
    gains = ((8, LANES), f32)
    qs, gs, kt, ku, qu, q_scale, e, sums, weighted, bias, gains = call(
        own_kernel,
        (query, key, value, out_grad, q_gain, k_gain, rel_bias),
        (stacked, stacked, turned, units, units, units, square, line, line,
         ((pairs, TILE, WIDE), f32), gains),
        scratch=[pltpu.VMEM(*hats)]
        + [pltpu.VMEM(*flat_low)] * 4
        + [pltpu.VMEM(q_gain.shape, f32), pltpu.VMEM(k_gain.shape, f32)]
        + [pltpu.VMEM(rel_bias.shape, f32), pltpu.SemaphoreType.DMA((7,))],
        hbm=7,
        flops=4_000_000_000,
    )
    krt, kru, er, norm, qn, dv, dv_before = call(
        before_kernel,
        (has_before, before_key, gains, qs, gs, e, sums, bias),
        (turned, units, square, line, stacked, flat, flat_low),
        scratch=[pltpu.VMEM(*hats), pltpu.VMEM((double, LANES), bf16)],
        scalars=1,
        flops=4_000_000_000,
    )
    dv_back = shifted(dv_before, "sp", -1)
    stat_rows = -(-(heads + 2) // 8) * 8
    members = (lax.axis_size("sp"), lax.axis_size("tp"))
    dq, dk, dk_before, stats = call(
        grad_kernel,
        (has_before, before_value, value, gs, qn, kt, krt, ku, kru, qu, q_scale, e, er, norm,
         weighted, gains),
        (flat_low, flat, flat_low, ((members[0] * members[1], stat_rows, LANES), f32)),
        scratch=[pltpu.VMEM(*square), pltpu.VMEM(*square)]
        + [pltpu.VMEM((pairs, 3, double), f32), pltpu.VMEM(*units)],
        scalars=1,
        flops=8_000_000_000,
    )
    dk_back = shifted(dk_before, "sp", -1)
    everyone = lax.all_to_all(stats, ("sp", "tp"), 0, 0, tiled=True)
    everyone = everyone.reshape(members + (stat_rows, LANES))
    dk, dv, q_gain_grad, k_gain_grad, bias_grad = call(
        final_kernel,
        (tp_index, gains, key, dk, dv, dk_back, dv_back, everyone),
        (flat_low, flat_low, ((1, head_width), f32), ((1, head_width), f32),
         ((heads, CLIP + 1), f32)),
        scalars=1,
        flops=1_000_000_000,
    )
    return (dq, dk, dv, q_gain_grad[0], k_gain_grad[0], bias_grad)


def solution(mesh):
    placed = (P("sp", "tp"), P("sp", "tp"), P("sp", "tp"), P("sp", "tp"), P(), P(), P("tp", None))
    return jax.shard_map(
        per_device,
        mesh=mesh,
        in_specs=placed,
        out_specs=(P("sp", "tp"), P("sp", "tp"), P("sp", "tp"), P(), P(), P("tp", None)),
        check_vma=False,
    )
```

time: 207 us -> 43.6 us (0.21)
  local copies, waits for them, and re-layouts: 72.1 us -> 0.01 us
  blocking collectives: 41.8 us -> 0 us
  matrix products: 35 us -> 0 us
  other arithmetic: 22.7 us -> 0 us
  Pallas kernels: 0 us -> 10.6 us
  starting transfers between devices: 10.9 us -> 20.8 us
  loops' own time: 5.63 us -> 0 us
  waiting for transfers between devices: 16.1 us -> 11.3 us
    reshape x12 -> x0, local copies, waits for them, and re-layouts: 43.3 us -> none  [the longest x4 16.2 us: tap_totals(): flattened = jnp.pad(widened.reshape(-1), (0, block))]
    psum x1 -> x0, blocking collectives: 41.8 us -> none  [per_device(): lax.psum((every_head, query_gain_part, key_gain_part), ('sp', 'tp'))]
    dot_general x24 -> x0, matrix products: 35 us -> none  [the longest x4 8.53 us: block_gradients(): jnp.dot(query_block, key_block.T, preferred_element_type=jnp.float32)]
    ppermute x4, waiting for transfers between devices: 16.1 us -> 3.02 us  [shifted(): return lax.ppermute(block, axis, route)]
    pad x4 -> x0, other arithmetic: 12 us -> none  [tap_totals(): flattened = jnp.pad(widened.reshape(-1), (0, block))]
    pallas_call x0 -> x4, Pallas kernels: none -> 10.6 us  [call(): pl.pallas_call(kernel, in_specs=specs, out_specs=[pl.BlockSpec(memory_spa...]
    all_to_all x0 -> x1, starting transfers between devices: none -> 9.86 us  [per_device(): everyone = lax.all_to_all(stats, ('sp', 'tp'), 0, 0, tiled=True)]
    another operation x8 -> x0, local copies, waits for them, and re-layouts: 8.97 us -> none  [bias_matrix(): flattened = jnp.tile(diagonal, block)[:block * (3 * block - 1)]]
  transfers between devices with their start and end apart: 4 -> 5, of which waited for: 4 -> 3; matrix products, arithmetic and copies ran while one was open for 2% -> 0% of each run, Pallas kernels for 0% -> 12%
where the time goes in v2:
time: 43.6 us; the launch traced here: 43.4 us
  starting transfers between devices  20.8 us (48%)
  waiting for transfers between devices  11.3 us (26%)
  Pallas kernels  10.6 us (24%)
  between operations  0.7 us (2%)
    ppermute x4, starting transfers between devices, shifted(): return lax.ppermute(block, axis, route)  10.9 us
    pallas_call x4, Pallas kernels, call(): pl.pallas_call(kernel, in_specs=specs, out_specs=[pl.BlockSpec(memory_spa...  10.6 us
    all_to_all x1, starting transfers between devices, per_device(): everyone = lax.all_to_all(stats, ('sp', 'tp'), 0, 0, tiled=True)  9.86 us
    all_to_all x1, waiting for transfers between devices, per_device(): everyone = lax.all_to_all(stats, ('sp', 'tp'), 0, 0, tiled=True)  8.28 us
    ppermute x4, waiting for transfers between devices, shifted(): return lax.ppermute(block, axis, route)  3.02 us
  transfers between devices with their start and end apart: 5, of which 3 were waited for; matrix products, arithmetic and copies ran while one was open for 0% of the time, Pallas kernels for 12%

profile of v2, /device:TPU:0, one launch (start us, length us, event | category | flops | bytes accessed | tf_op | source)
XLA Modules:
  0.0 43.4 jit_solution(1524175760916429094)
XLA Ops:
  0.6 4.9 %collective-permute-start.1 = (bf16[512,256]{1,0:T(8,128)(2,1)}, bf16[512,256]{1,0:T(8,128)(2,1)S(1)}, u32[]{:S(2)}, u32[]{:S(2)}) collective-permute-start(bf16[512,256]{1,0:T(8,128)(2,1)} %k_ref.1), channel_id=1, source_target_pairs={{0,4},{4,8},{8,12},{12,16},{16,20},{20,24},{24,28},{1,5},{5,9},{9,... | collective-permute-start | bytes 786440 | tf_op jit(solution)/shard_map/ppermute | solution.py:26
  5.6 3.4 %collective-permute-start = (bf16[512,256]{1,0:T(8,128)(2,1)}, bf16[512,256]{1,0:T(8,128)(2,1)S(1)}, u32[]{:S(2)}, u32[]{:S(2)}) collective-permute-start(bf16[512,256]{1,0:T(8,128)(2,1)} %v_ref.1), channel_id=1, source_target_pairs={{0,4},{4,8},{8,12},{12,16},{16,20},{20,24},{24,28},{1,5},{5,9},{9,... | collective-permute-start | bytes 786440 | tf_op jit(solution)/shard_map/ppermute | solution.py:26
  9.0 2.8 %shard_map.118 = (bf16[2,1024,128]{2,1,0:T(8,128)(2,1)S(1)}, bf16[2,1024,128]{2,1,0:T(8,128)(2,1)S(1)}, bf16[2,128,512]{2,1,0:T(8,128)(2,1)S(1)}, f32[2,512,128]...) custom-call(bf16[512,256]{1,0:T(8,128)(2,1)} %q_hbm.1, ...), custom_call_target="tpu_custom_call" | custom-call | flops 4000000000 | tf_op jit(solution)/shard_map/pallas_call | solution.py:387
  11.8 0.7 %collective-permute-done.1.kr_ref = bf16[512,256]{1,0:T(8,128)(2,1)S(1)} collective-permute-done((bf16[512,256]{1,0:T(8,128)(2,1)}, bf16[512,256]{1,0:T(8,128)(2,1)S(1)}, u32[]{:S(2)}, u32[]{:S(2)}) %collective-permute-start.1) | collective-permute-done | bytes 262176 | tf_op jit(solution)/shard_map/ppermute | solution.py:26
  12.5 0.0 copy-start
  12.5 2.2 %shard_map.119 = (bf16[2,128,512]{2,1,0:T(8,128)(2,1)S(1)}, f32[2,512,128]{2,1,0:T(8,128)S(1)}, bf16[2,512,1024]{2,1,0:T(8,128)(2,1)S(1)}, f32[2,8,1024]{2,1,0:T...) custom-call(s32[1]{0:T(128)} %bitcast.has_before, ...), custom_call_target="tpu_custom_call" | custom-call | flops 4000000000 | tf_op jit(solution)/shard_map/pallas_call | solution.py:387
  14.7 2.3 %collective-permute-done.vr_ref = bf16[512,256]{1,0:T(8,128)(2,1)S(1)} collective-permute-done((bf16[512,256]{1,0:T(8,128)(2,1)}, bf16[512,256]{1,0:T(8,128)(2,1)S(1)}, u32[]{:S(2)}, u32[]{:S(2)}) %collective-permute-start) | collective-permute-done | bytes 262176 | tf_op jit(solution)/shard_map/ppermute | solution.py:26
  17.0 0.0 copy-done
  17.0 0.0 copy-start.1
  17.0 4.1 %shard_map.120 = (bf16[512,256]{1,0:T(8,128)(2,1)}, f32[512,256]{1,0:T(8,128)S(1)}, bf16[512,256]{1,0:T(8,128)(2,1)S(1)}, f32[32,8,128]{2,1,0:T(8,128)}) custom-call(s32[1]{0:T(128)} %bitcast.has_before, bf16[512,256]{1,0:T(8,128)(2,1)S(1)} %collective-permute-done.vr_ref, bf16[512,256]{1,0:T(8,128)(2,1)S(1)} %copy-done, ...), custom_call_target="tpu_custom_call" | custom-call | flops 8000000000 | tf_op jit(solution)/shard_map/pallas_call | solution.py:387
  21.2 1.3 %collective-permute-start.2 = (bf16[512,256]{1,0:T(8,128)(2,1)S(1)}, bf16[512,256]{1,0:T(8,128)(2,1)S(1)}, u32[]{:S(2)}, u32[]{:S(2)}) collective-permute-start(bf16[512,256]{1,0:T(8,128)(2,1)S(1)} %get-tuple-element.52), channel_id=1, source_target_pairs={{4,0},{8,4},{12,8},{16,12},{20,16},{24,20},{28,24},{5,1},{9,5},{13... | collective-permute-start | bytes 786440 | tf_op jit(solution)/shard_map/ppermute | solution.py:26
  22.5 1.3 %collective-permute-start.3 = (bf16[512,256]{1,0:T(8,128)(2,1)S(1)}, bf16[512,256]{1,0:T(8,128)(2,1)S(1)}, u32[]{:S(2)}, u32[]{:S(2)}) collective-permute-start(bf16[512,256]{1,0:T(8,128)(2,1)S(1)} %get-tuple-element.53), channel_id=1, source_target_pairs={{4,0},{8,4},{12,8},{16,12},{20,16},{24,20},{28,24},{5,1},{9,5},{13... | collective-permute-start | bytes 786440 | tf_op jit(solution)/shard_map/ppermute | solution.py:26
  23.8 9.9 %all-to-all-start = ((f32[32,8,128]{2,1,0:T(8,128)}), f32[32,8,128]{2,1,0:T(8,128)S(1)}, u32[]{:S(2)}, u32[]{:S(2)}) async-start(f32[32,8,128]{2,1,0:T(8,128)} %get-tuple-element.54), calls=%async_computation | async-start | bytes 262144 | tf_op jit(solution)/shard_map/all_to_all | solution.py:451
  33.6 8.3 %all-to-all-done = f32[32,8,128]{2,1,0:T(8,128)S(1)} async-done(((f32[32,8,128]{2,1,0:T(8,128)}), f32[32,8,128]{2,1,0:T(8,128)S(1)}, u32[]{:S(2)}, u32[]{:S(2)}) %all-to-all-start) | async-done | bytes 131104 | tf_op jit(solution)/shard_map/all_to_all | solution.py:451
  41.9 0.0 collective-permute-done.2.dkb_ref
  41.9 0.0 collective-permute-done.3.dvb_ref
  41.9 0.0 copy-done.1
  41.9 1.4 %shard_map.121 = (bf16[512,256]{1,0:T(8,128)(2,1)}, bf16[512,256]{1,0:T(8,128)(2,1)}, f32[1,64]{1,0:T(1,128)}, f32[1,64]{1,0:T(1,128)}, f32[4,129]{1,0:T(4,128)}) custom-call(s32[1]{0:T(128)} %bitcast.3.tp_index, f32[8,128]{1,0:T(8,128)S(1)} %get-tuple-element.34.gains_ref, bf16[512,256]{1,0:T(8,128)(2,1)S(1)} %copy-done.1, ...), custom_call_target="tpu_custom_call" | custom-call | flops 1000000000 | tf_op jit(solution)/shard_map/pallas_call | solution.py:387
Async XLA Ops:
  0.6 11.9 %collective-permute-start.1 = (bf16[512,256]{1,0:T(8,128)(2,1)}, bf16[512,256]{1,0:T(8,128)(2,1)S(1)}, u32[]{:S(2)}, u32[]{:S(2)}) collective-permute-start(bf16[512,256]{1,0:T(8,128)(2,1)} %k_ref.1), channel_id=1, source_target_pairs={{0,4},{4,8},{8,12},{12,16},{16,20},{20,24},{24,28},{1,5},{5,9},{9,... | collective-permute-start | bytes 786440 | tf_op jit(solution)/shard_map/ppermute | solution.py:26
  5.6 11.5 %collective-permute-start = (bf16[512,256]{1,0:T(8,128)(2,1)}, bf16[512,256]{1,0:T(8,128)(2,1)S(1)}, u32[]{:S(2)}, u32[]{:S(2)}) collective-permute-start(bf16[512,256]{1,0:T(8,128)(2,1)} %v_ref.1), channel_id=1, source_target_pairs={{0,4},{4,8},{8,12},{12,16},{16,20},{20,24},{24,28},{1,5},{5,9},{9,... | collective-permute-start | bytes 786440 | tf_op jit(solution)/shard_map/ppermute | solution.py:26
  12.5 4.5 %copy-start = (bf16[512,256]{1,0:T(8,128)(2,1)S(1)}, bf16[512,256]{1,0:T(8,128)(2,1)}, u32[]{:S(2)}) copy-start(bf16[512,256]{1,0:T(8,128)(2,1)} %v_ref.1) | copy-start | bytes 786436
  17.0 24.9 %copy-start.1 = (bf16[512,256]{1,0:T(8,128)(2,1)S(1)}, bf16[512,256]{1,0:T(8,128)(2,1)}, u32[]{:S(2)}) copy-start(bf16[512,256]{1,0:T(8,128)(2,1)} %k_ref.1) | copy-start | bytes 786436
  21.2 20.7 %collective-permute-start.2 = (bf16[512,256]{1,0:T(8,128)(2,1)S(1)}, bf16[512,256]{1,0:T(8,128)(2,1)S(1)}, u32[]{:S(2)}, u32[]{:S(2)}) collective-permute-start(bf16[512,256]{1,0:T(8,128)(2,1)S(1)} %get-tuple-element.52), channel_id=1, source_target_pairs={{4,0},{8,4},{12,8},{16,12},{20,16},{24,20},{28,24},{5,1},{9,5},{13... | collective-permute-start | bytes 786440 | tf_op jit(solution)/shard_map/ppermute | solution.py:26
  22.5 19.5 %collective-permute-start.3 = (bf16[512,256]{1,0:T(8,128)(2,1)S(1)}, bf16[512,256]{1,0:T(8,128)(2,1)S(1)}, u32[]{:S(2)}, u32[]{:S(2)}) collective-permute-start(bf16[512,256]{1,0:T(8,128)(2,1)S(1)} %get-tuple-element.53), channel_id=1, source_target_pairs={{4,0},{8,4},{12,8},{16,12},{20,16},{24,20},{28,24},{5,1},{9,5},{13... | collective-permute-start | bytes 786440 | tf_op jit(solution)/shard_map/ppermute | solution.py:26
  23.8 18.2 %all-to-all-start = ((f32[32,8,128]{2,1,0:T(8,128)}), f32[32,8,128]{2,1,0:T(8,128)S(1)}, u32[]{:S(2)}, u32[]{:S(2)}) async-start(f32[32,8,128]{2,1,0:T(8,128)} %get-tuple-element.54), calls=%async_computation | async-start | bytes 262144 | tf_op jit(solution)/shard_map/all_to_all | solution.py:451

commit v3 on v2

v3 whole, which is shorter than its diff:
```python
import jax
import jax.numpy as jnp
from jax import lax
from jax.experimental import pallas as pl
from jax.experimental.pallas import tpu as pltpu
from jax.sharding import PartitionSpec as P


SEG = 64
CLIP = 128
LANES = 128
TILE = 128
WIDE = 2 * TILE
GRANT = 16 * 1024 * 1024

epsilon = 1e-06
f32 = jnp.float32
bf16 = jnp.bfloat16

ROWS_COLS = (((1,), (1,)), ((), ()))


def shifted(block, axis, distance):
    devices = range(lax.axis_size(axis))
    route = [(i - distance, i) for i in devices if i - distance in devices]
    return lax.ppermute(block, axis, route)


def iota(shape, dim):
    return lax.broadcasted_iota(jnp.int32, shape, dim)


def split_dot(x, matrix):
    high = x.astype(bf16)
    low = (x - high.astype(f32)).astype(bf16)
    return jnp.dot(high, matrix, preferred_element_type=f32) + jnp.dot(
        low, matrix, preferred_element_type=f32
    )


def head_mean(x, head_width):
    same = iota((LANES, LANES), 0) // head_width == iota((LANES, LANES), 1) // head_width
    return split_dot(x, jnp.where(same, 1.0 / head_width, 0.0).astype(bf16))


def unit_and_scale(rows, head_width):
    widened = rows.astype(f32)
    scale = lax.rsqrt(head_mean(widened * widened, head_width) + epsilon)
    return widened * scale, scale


def norm_backward(grad_hat, unit, scale, gain, head_width):
    grad_unit = grad_hat * gain
    inner = head_mean(grad_unit * unit, head_width)
    return scale * (grad_unit - unit * inner)


def rows8(x):
    return jnp.sum(x.reshape(x.shape[0] // 8, 8, x.shape[1]), axis=0)


def both_heads(gain_ref):
    gain = gain_ref[...]
    return jnp.concatenate([gain] * (LANES // gain.shape[1]), axis=1)


def each_pair(pairs, body):
    for p in range(pairs):
        body(p)


def at(tile):
    return pl.ds(tile * TILE, TILE)


def masks():
    key_pos = iota((TILE, WIDE), 0)
    query_pos = iota((TILE, WIDE), 1) % TILE
    return query_pos >= key_pos, key_pos // SEG >= query_pos // SEG


def as_column(row, rows):
    turned = jnp.broadcast_to(row, (LANES, rows)).T
    return turned


def own_kernel(
    q_hbm, k_hbm, v_hbm, g_hbm, q_gain_hbm, k_gain_hbm, table_hbm,
    qs_ref, gs_ref, kt_ref, qu_ref, e_ref, e32_ref, d32_ref, sum_ref, weighted_ref,
    bias_ref, gains_ref, kh_ref, q_ref, k_ref, v_ref, g_ref, q_gain_ref, k_gain_ref, table_ref, sems,
):
    sources = (q_gain_hbm, k_gain_hbm, table_hbm, k_hbm, q_hbm, g_hbm, v_hbm)
    targets = (q_gain_ref, k_gain_ref, table_ref, k_ref, q_ref, g_ref, v_ref)
    copies = [
        pltpu.make_async_copy(source, target, sems.at[i])
        for i, (source, target) in enumerate(zip(sources, targets))
    ]
    for copy in copies:
        copy.start()
    for copy in copies:
        copy.wait()
    rows = q_ref.shape[0]
    tiles = rows // TILE
    head_width = q_gain_ref.shape[1]
    q_gain, k_gain = both_heads(q_gain_ref), both_heads(k_gain_ref)
    gains_ref[...] = jnp.concatenate([q_gain, k_gain, jnp.zeros((6, LANES), f32)], axis=0)
    causal, _ = masks()
    first = iota((TILE, LANES), 1) < head_width
    zero = jnp.zeros((TILE, LANES), bf16)
    table = table_ref[...]
    near = table[:, :CLIP] - table[:, CLIP:]

    def body(p):
        lanes = pl.ds(p * LANES, LANES)
        unit, _ = unit_and_scale(k_ref[:, lanes], head_width)
        hat = (unit * k_gain).astype(bf16)
        kh_ref[p] = hat
        kt_ref[p] = hat.T
        unit, _ = unit_and_scale(q_ref[:, lanes], head_width)
        qu_ref[p] = unit
        hat = (unit * q_gain).astype(bf16) * jnp.asarray(head_width ** (-0.5), bf16)
        for b in range(tiles):
            part = hat[b * TILE : (b + 1) * TILE, :]
            grad = g_ref[at(b), lanes]
            qs_ref[p, pl.ds(b * WIDE, TILE), :] = jnp.where(first, part, zero)
            qs_ref[p, pl.ds(b * WIDE + TILE, TILE), :] = jnp.where(first, zero, part)
            gs_ref[p, pl.ds(b * WIDE, TILE), :] = jnp.where(first, grad, zero)
            gs_ref[p, pl.ds(b * WIDE + TILE, TILE), :] = jnp.where(first, zero, grad)
        skewed = [
            pltpu.roll(
                jnp.broadcast_to(near[2 * p + h : 2 * p + h + 1, :], (TILE, TILE)),
                0,
                1,
                stride=1,
                stride_axis=0,
            )
            for h in range(2)
        ]
        bias = jnp.concatenate(skewed, axis=1)
        below = jnp.where(causal, 0.0, bias)
        bias_ref[p] = below
        for b in range(tiles):
            queries = pl.ds(b * WIDE, WIDE)
            q_tile, g_tile = qs_ref[p, queries, :], gs_ref[p, queries, :]
            total = jnp.zeros((8, WIDE), f32)
            weighted = jnp.zeros((8, WIDE), f32)
            for a in range(b + 1):
                scores = lax.dot_general(
                    kh_ref[p, at(a), :], q_tile, ROWS_COLS, preferred_element_type=f32
                )
                if a == b:
                    scores = scores + bias
                if a == b - 1:
                    scores = scores + below
                e = jnp.exp(scores)
                if a == b:
                    e = jnp.where(causal, e, 0.0)
                d = lax.dot_general(
                    v_ref[at(a), lanes], g_tile, ROWS_COLS, preferred_element_type=f32
                )
                total = total + rows8(e)
                weighted = weighted + rows8(e * d)
                e_ref[p, at(a), queries] = e.astype(bf16)
                e32_ref[p, at(a), queries] = e
                d32_ref[p, at(a), queries] = d
            sum_ref[p, :, queries] = total
            weighted_ref[p, :, queries] = weighted

    each_pair(qs_ref.shape[0], body)


def before_kernel(
    has_before, kr_ref, gains_ref, qs_ref, gs_ref, kt_ref, e_ref, sum_ref, bias_ref,
    kts_ref, er32_ref, norm_ref, qn_ref, dv_ref, dvr_ref, krh_ref, gn_ref, er_ref,
):
    rows, width = kr_ref.shape
    tiles = rows // TILE
    head_width = width // (2 * qs_ref.shape[0])
    before = has_before[0].astype(f32)
    k_gain = gains_ref[1:2, :]
    _, inside = masks()

    def body(p):
        lanes = pl.ds(p * LANES, LANES)
        unit, _ = unit_and_scale(kr_ref[:, lanes], head_width)
        hat = (unit * k_gain).astype(bf16)
        krh_ref[p] = hat
        kts_ref[p, :, :rows] = hat.T
        kts_ref[p, :, rows:] = kt_ref[p]
        for b in range(tiles):
            queries = pl.ds(b * WIDE, WIDE)
            q_tile = qs_ref[p, queries, :]
            total = jnp.zeros((8, WIDE), f32)
            for a in range(b, tiles):
                scores = lax.dot_general(
                    krh_ref[p, at(a), :], q_tile, ROWS_COLS, preferred_element_type=f32
                )
                if b == 0 and a == tiles - 1:
                    scores = scores + bias_ref[p]
                e = jnp.exp(scores)
                if a == b:
                    e = jnp.where(inside, e, 0.0)
                total = total + rows8(e)
                er_ref[p, at(a), queries] = e.astype(bf16)
                er32_ref[p, at(a), queries] = e
            normalizer = jnp.sum(
                sum_ref[p, :, queries] + total * before, axis=0, keepdims=True
            )
            norm_ref[p, :, queries] = jnp.broadcast_to(normalizer, (8, WIDE))
            column = as_column(1.0 / normalizer, WIDE)
            qn_ref[p, queries, :] = (q_tile.astype(f32) * column).astype(bf16)
            gn_ref[queries, :] = (gs_ref[p, queries, :].astype(f32) * column).astype(bf16)
        for a in range(tiles):
            span = pl.ds(0, (a + 1) * WIDE)
            dvr_ref[at(a), lanes] = jnp.dot(
                er_ref[p, at(a), span], gn_ref[span, :], preferred_element_type=f32
            ).astype(bf16)
        for a in range(tiles):
            span = pl.ds(a * WIDE, (tiles - a) * WIDE)
            dv_ref[at(a), lanes] = jnp.dot(
                e_ref[p, at(a), span], gn_ref[span, :], preferred_element_type=f32
            )

    each_pair(qs_ref.shape[0], body)


def grad_kernel(
    has_before, vr_ref, dd_ref, gs_ref, qn_ref, kts_ref, qu_ref, e_ref, er_ref, norm_ref,
    weighted_ref,
    dq_ref, dk_ref, dkr_ref, stats_hbm, s_ref, d_ref, delta_ref, table_ref, sem,
):
    rows, width = vr_ref.shape
    tiles = rows // TILE
    pairs = qn_ref.shape[0]
    heads = 2 * pairs
    head_width = width // heads
    before = has_before[0].astype(f32)
    causal, _ = masks()
    one_lane = iota((1, LANES), 1)
    always = has_before[0] > -1
    still = has_before[0] > -2

    @pl.when(always)
    def _():
        for p in range(pairs):
            lanes = pl.ds(p * LANES, LANES)
            for b in range(tiles):
                queries = pl.ds(b * WIDE, WIDE)
                g_tile = gs_ref[p, queries, :]
                weighted = weighted_ref[p, :, queries]
                for a in range(b, tiles):
                    d = lax.dot_general(
                        vr_ref[at(a), lanes], g_tile, ROWS_COLS, preferred_element_type=f32
                    )
                    d_ref[p, at(a), queries] = d
                    weighted = weighted + rows8(er_ref[p, at(a), queries] * d)
                weighted = jnp.sum(weighted, axis=0, keepdims=True)
                normalizer = norm_ref[p, 0:1, queries]
                inverse = 1.0 / normalizer
                delta = weighted * inverse
                rest = (weighted - delta * normalizer) * inverse
                delta_ref[p, :, queries] = jnp.concatenate([inverse, delta, rest], axis=0)

    @pl.when(still)
    def _():
        for p in range(pairs):
            lanes = pl.ds(p * LANES, LANES)
            for b in range(tiles):
                queries = pl.ds(b * WIDE, WIDE)
                delta = delta_ref[p, 1:2, queries]
                for a in range(b, tiles):
                    s = er_ref[p, at(a), queries] * (d_ref[p, at(a), queries] - delta)
                    s_ref[p, at(a), queries] = s.astype(bf16)
                for a in range(b + 1):
                    s = e_ref[p, at(a), queries] * (dd_ref[p, at(a), queries] - delta)
                    s_ref[p, at(tiles + a), queries] = s.astype(bf16)

    @pl.when(still)
    def _():
        for p in range(pairs):
            for b in range(tiles):
                queries = pl.ds(b * WIDE, WIDE)
                span = pl.ds(b * TILE, rows + TILE)
                turned = jnp.dot(
                    kts_ref[p, :, span], s_ref[p, span, queries], preferred_element_type=f32
                )
                turned = jnp.concatenate(
                    [turned[:head_width, :TILE], turned[head_width:, TILE:]], axis=0
                )
                inverse = delta_ref[p, 0:1, queries] * head_width ** (-0.5)
                inverse = jnp.concatenate(
                    [
                        jnp.broadcast_to(inverse[:, :TILE], (head_width, TILE)),
                        jnp.broadcast_to(inverse[:, TILE:], (head_width, TILE)),
                    ],
                    axis=0,
                )
                dq_ref[p, at(b), :] = (turned * inverse).T

    @pl.when(still)
    def _():
        q_sum = jnp.zeros((8, LANES), f32)
        for p in range(pairs):
            q_sum = q_sum + rows8(dq_ref[p] * qu_ref[p])
        q_sum = jnp.sum(q_sum, axis=0, keepdims=True)
        flip = iota((TILE, TILE), 0) + iota((TILE, TILE), 1) == TILE - 1
        flip = jnp.where(flip, 1.0, 0.0).astype(bf16)
        lines = []
        last = jnp.zeros((1, LANES), f32)
        for p in range(pairs):
            near_grad = jnp.zeros((TILE, WIDE), f32)
            total = jnp.zeros((1, WIDE), f32)
            for b in range(tiles):
                queries = pl.ds(b * WIDE, WIDE)
                total = total + delta_ref[p, 2:3, queries]
                below = s_ref[p, at(tiles + b - 1), queries].astype(f32)
                if b == 0:
                    below = below * before
                both = jnp.where(causal, s_ref[p, at(tiles + b), queries].astype(f32), below)
                near_grad = near_grad + both * delta_ref[p, 0:1, queries]
            near_grad = split_dot_left(flip, near_grad)
            for h in range(2):
                half = slice(h * TILE, (h + 1) * TILE)
                straight = pltpu.roll(near_grad[:, half], 1, 1, stride=1, stride_axis=0)
                taps = jnp.sum(straight, axis=0, keepdims=True)
                lines.append(taps)
                rest = jnp.sum(total[:, half] - taps, axis=1, keepdims=True)
                last = last + jnp.where(one_lane == 2 * p + h, rest, 0.0)
        lines += high_and_low(q_sum + pltpu.roll(q_sum, head_width, 1))
        lines += high_and_low(last)
        empty = table_ref.shape[1] - len(lines)
        if empty:
            lines.append(jnp.zeros((empty, LANES), f32))
        table = jnp.concatenate(lines, axis=0).astype(bf16)
        table_ref[...] = jnp.broadcast_to(table[None], table_ref.shape)

    copy = pltpu.make_async_copy(table_ref, stats_hbm, sem)
    copy.start()
    for p in range(pairs):
        lanes = pl.ds(p * LANES, LANES)
        for a in range(2 * tiles):
            low, high = max(0, a - tiles), min(tiles - 1, a)
            span = pl.ds(low * WIDE, (high - low + 1) * WIDE)
            dk = jnp.dot(s_ref[p, at(a), span], qn_ref[p, span, :], preferred_element_type=f32)
            if a < tiles:
                dkr_ref[at(a), lanes] = dk.astype(bf16)
            else:
                dk_ref[p, at(a - tiles), :] = dk
    copy.wait()


def high_and_low(x):
    high = x.astype(bf16).astype(f32)
    return [high, x - high]


def split_dot_left(matrix, x):
    high = x.astype(bf16)
    low = (x - high.astype(f32)).astype(bf16)
    return jnp.dot(matrix, high, preferred_element_type=f32) + jnp.dot(
        matrix, low, preferred_element_type=f32
    )


def finish_kernel(
    gains_ref, dqh_ref, q_ref, k_ref, dk_ref, dv_ref, dkb_ref, dvb_ref, dq_out, dk_out, dv_out
):
    pairs = dqh_ref.shape[0]
    head_width = k_ref.shape[1] // (2 * pairs)
    q_gain, k_gain = gains_ref[0:1, :], gains_ref[1:2, :]

    def body(p):
        lanes = pl.ds(p * LANES, LANES)
        unit, scale = unit_and_scale(q_ref[:, lanes], head_width)
        dq_out[:, lanes] = norm_backward(dqh_ref[p], unit, scale, q_gain, head_width).astype(bf16)
        unit, scale = unit_and_scale(k_ref[:, lanes], head_width)
        grad_hat = dk_ref[p] + dkb_ref[:, lanes].astype(f32)
        dk_out[:, lanes] = norm_backward(grad_hat, unit, scale, k_gain, head_width).astype(bf16)
        dv_out[:, lanes] = (dv_ref[:, lanes] + dvb_ref[:, lanes].astype(f32)).astype(bf16)

    each_pair(pairs, body)


def total_kernel(tp_index, gains_ref, all_ref, q_gain_out, k_gain_out, bias_out):
    heads = bias_out.shape[0]
    head_width = q_gain_out.shape[1]
    everyone = jnp.sum(all_ref[...].astype(f32), axis=0)
    gains = jnp.sum(everyone[:, heads : heads + 2, :], axis=0)
    gains = gains[0:1, :] + gains[1:2, :]
    q_gain_out[...] = gains[:, :head_width]
    ratio = gains_ref[0:1, :head_width] / gains_ref[1:2, :head_width]
    k_gain_out[...] = gains[:, :head_width] * ratio
    mine = iota(everyone.shape, 0) == tp_index[0]
    summed = jnp.sum(jnp.where(mine, everyone, 0.0), axis=0)
    bias_out[:, :CLIP] = summed[:heads, :]
    last = summed[heads + 2 : heads + 3, :] + summed[heads + 3 : heads + 4, :]
    diagonal = iota((heads, LANES), 0) == iota((heads, LANES), 1)
    bias_out[:, CLIP:] = jnp.sum(jnp.where(diagonal, last, 0.0), axis=1, keepdims=True)


def call(kernel, args, outs, scratch=(), scalars=0, hbm=0, out_hbm=(), flops=0):
    args = [
        pltpu.with_memory_space_constraint(x, pltpu.HBM) if scalars <= i < scalars + hbm else x
        for i, x in enumerate(args)
    ]
    specs = [pl.BlockSpec(memory_space=pltpu.SMEM)] * scalars
    specs += [pl.BlockSpec(memory_space=pltpu.HBM)] * hbm
    specs += [pl.BlockSpec(memory_space=pltpu.VMEM)] * (len(args) - scalars - hbm)
    return pl.pallas_call(
        kernel,
        in_specs=specs,
        out_specs=[
            pl.BlockSpec(memory_space=pltpu.HBM if i in out_hbm else pltpu.VMEM)
            for i in range(len(outs))
        ],
        out_shape=[jax.ShapeDtypeStruct(*o) for o in outs],
        scratch_shapes=list(scratch),
        compiler_params=pltpu.CompilerParams(vmem_limit_bytes=GRANT),
        cost_estimate=pl.CostEstimate(flops=flops, bytes_accessed=0, transcendentals=0),
    )(*args)


def per_device(query, key, value, out_grad, query_gain, key_gain, rel_bias):
    rows, width = query.shape
    heads = rel_bias.shape[0]
    head_width = width // heads
    pairs = width // LANES
    double = 2 * rows
    before_key = shifted(key, "sp", 1)
    before_value = shifted(value, "sp", 1)
    q_gain, k_gain = query_gain[None, :], key_gain[None, :]
    has_before = (lax.axis_index("sp") > 0).astype(jnp.int32).reshape(1)
    tp_index = lax.axis_index("tp").astype(jnp.int32).reshape(1)
    stacked = ((pairs, double, LANES), bf16)
    hats = ((pairs, rows, LANES), bf16)
    turned = ((pairs, LANES, rows), bf16)
    units = ((pairs, rows, LANES), f32)
    square = ((pairs, rows, double), bf16)
    square32 = ((pairs, rows, double), f32)
    line = ((pairs, 8, double), f32)
    flat, flat_low = ((rows, width), f32), ((rows, width), bf16)
    gains = ((8, LANES), f32)
    qs, gs, kt, qu, e, e32, d32, sums, weighted, bias, gains = call(
        own_kernel,
        (query, key, value, out_grad, q_gain, k_gain, rel_bias),
        (stacked, stacked, turned, units, square, square32, square32, line, line,
         ((pairs, TILE, WIDE), f32), gains),
        scratch=[pltpu.VMEM(*hats)]
        + [pltpu.VMEM(*flat_low)] * 4
        + [pltpu.VMEM(q_gain.shape, f32), pltpu.VMEM(k_gain.shape, f32)]
        + [pltpu.VMEM(rel_bias.shape, f32), pltpu.SemaphoreType.DMA((7,))],
        hbm=7,
        flops=4_000_000_000,
    )
    kts, er32, norm, qn, dv, dv_before = call(
        before_kernel,
        (has_before, before_key, gains, qs, gs, kt, e, sums, bias),
        (((pairs, LANES, double), bf16), square32, line, stacked, flat, flat_low),
        scratch=[pltpu.VMEM(*hats), pltpu.VMEM((double, LANES), bf16), pltpu.VMEM(*square)],
        scalars=1,
        flops=4_000_000_000,
    )
    dv_back = shifted(dv_before, "sp", -1)
    stat_rows = -(-(heads + 4) // 8) * 8
    members = (lax.axis_size("sp"), lax.axis_size("tp"))
    spread = ((members[0] * members[1], stat_rows, LANES), bf16)
    dq_hat, dk, dk_before, stats = call(
        grad_kernel,
        (has_before, before_value, d32, gs, qn, kts, qu, e32, er32, norm, weighted),
        (units, units, flat_low, spread),
        out_hbm=(3,),
        scratch=[pltpu.VMEM((pairs, double, double), bf16), pltpu.VMEM(*square32)]
        + [pltpu.VMEM((pairs, 3, double), f32), pltpu.VMEM(*spread), pltpu.SemaphoreType.DMA],
        scalars=1,
        flops=8_000_000_000,
    )
    dk_back = shifted(dk_before, "sp", -1)
    everyone = lax.all_to_all(stats, ("sp", "tp"), 0, 0, tiled=True)
    everyone = everyone.reshape(members + (stat_rows, LANES))
    dq, dk, dv = call(
        finish_kernel,
        (gains, dq_hat, query, key, dk, dv, dk_back, dv_back),
        (flat_low, flat_low, flat_low),
        flops=1_000_000_000,
    )
    q_gain_grad, k_gain_grad, bias_grad = call(
        total_kernel,
        (tp_index, gains, everyone),
        (((1, head_width), f32), ((1, head_width), f32), ((heads, CLIP + 1), f32)),
        scalars=1,
        flops=1_000_000,
    )
    return (dq, dk, dv, q_gain_grad[0], k_gain_grad[0], bias_grad)


def solution(mesh):
    placed = (P("sp", "tp"), P("sp", "tp"), P("sp", "tp"), P("sp", "tp"), P(), P(), P("tp", None))
    return jax.shard_map(
        per_device,
        mesh=mesh,
        in_specs=placed,
        out_specs=(P("sp", "tp"), P("sp", "tp"), P("sp", "tp"), P(), P(), P("tp", None)),
        check_vma=False,
    )
```

time: 43.6 us -> 42.8 us (0.982)
  waiting for transfers between devices: 11.3 us -> 10.6 us
    all_to_all x1, waiting for transfers between devices: 8.28 us -> 7.63 us  [per_device(): everyone = lax.all_to_all(stats, ('sp', 'tp'), 0, 0, tiled=True)]
    pallas_call x4 -> x5, Pallas kernels: 10.6 us -> 10.4 us  [call(): pl.pallas_call(kernel, in_specs=specs, out_specs=[pl.BlockSpec(memory_spa...]
  transfers between devices with their start and end apart: 5 -> 5, of which waited for: 3 -> 3; matrix products, arithmetic and copies ran while one was open for 0% -> 0% of each run, Pallas kernels for 12% -> 14%
where the time goes in v3:
time: 42.8 us; the launch traced here: 42.5 us
  starting transfers between devices  20.8 us (49%)
  waiting for transfers between devices  10.6 us (25%)
  Pallas kernels  10.4 us (24%)
  between operations  0.72 us (2%)
    ppermute x4, starting transfers between devices, shifted(): return lax.ppermute(block, axis, route)  10.9 us
    pallas_call x5, Pallas kernels, call(): pl.pallas_call(kernel, in_specs=specs, out_specs=[pl.BlockSpec(memory_spa...  10.4 us
    all_to_all x1, starting transfers between devices, per_device(): everyone = lax.all_to_all(stats, ('sp', 'tp'), 0, 0, tiled=True)  9.87 us
    all_to_all x1, waiting for transfers between devices, per_device(): everyone = lax.all_to_all(stats, ('sp', 'tp'), 0, 0, tiled=True)  7.63 us
    ppermute x4, waiting for transfers between devices, shifted(): return lax.ppermute(block, axis, route)  2.95 us
  transfers between devices with their start and end apart: 5, of which 3 were waited for; matrix products, arithmetic and copies ran while one was open for 0% of the time, Pallas kernels for 14%

profile of v3, /device:TPU:0, one launch (start us, length us, event | category | flops | bytes accessed | tf_op | source)
XLA Modules:
  0.0 42.5 jit_solution(16647362096388686440)
XLA Ops:
  0.6 4.9 %collective-permute-start.1 = (bf16[512,256]{1,0:T(8,128)(2,1)}, bf16[512,256]{1,0:T(8,128)(2,1)S(1)}, u32[]{:S(2)}, u32[]{:S(2)}) collective-permute-start(bf16[512,256]{1,0:T(8,128)(2,1)} %k_ref.1), channel_id=1, source_target_pairs={{0,4},{4,8},{8,12},{12,16},{16,20},{20,24},{24,28},{1,5},{5,9},{9,... | collective-permute-start | bytes 786440 | tf_op jit(solution)/shard_map/ppermute | solution.py:26
  5.6 3.4 %collective-permute-start = (bf16[512,256]{1,0:T(8,128)(2,1)}, bf16[512,256]{1,0:T(8,128)(2,1)S(1)}, u32[]{:S(2)}, u32[]{:S(2)}) collective-permute-start(bf16[512,256]{1,0:T(8,128)(2,1)} %v_hbm.1), channel_id=1, source_target_pairs={{0,4},{4,8},{8,12},{12,16},{16,20},{20,24},{24,28},{1,5},{5,9},{9,... | collective-permute-start | bytes 786440 | tf_op jit(solution)/shard_map/ppermute | solution.py:26
  9.0 2.9 %shard_map.118 = (bf16[2,1024,128]{2,1,0:T(8,128)(2,1)S(1)}, bf16[2,1024,128]{2,1,0:T(8,128)(2,1)S(1)}, bf16[2,128,512]{2,1,0:T(8,128)(2,1)S(1)}, f32[2,512,128]...) custom-call(bf16[512,256]{1,0:T(8,128)(2,1)} %q_ref.1, ...), custom_call_target="tpu_custom_call" | custom-call | flops 4000000000 | tf_op jit(solution)/shard_map/pallas_call | solution.py:409
  11.9 0.6 %collective-permute-done.1.kr_ref = bf16[512,256]{1,0:T(8,128)(2,1)S(1)} collective-permute-done((bf16[512,256]{1,0:T(8,128)(2,1)}, bf16[512,256]{1,0:T(8,128)(2,1)S(1)}, u32[]{:S(2)}, u32[]{:S(2)}) %collective-permute-start.1) | collective-permute-done | bytes 262176 | tf_op jit(solution)/shard_map/ppermute | solution.py:26
  12.5 2.2 %shard_map.119 = (bf16[2,128,1024]{2,1,0:T(8,128)(2,1)S(1)}, f32[2,512,1024]{2,1,0:T(8,128)S(1)}, f32[2,8,1024]{2,1,0:T(8,128)S(1)}, bf16[2,1024,128]{2,1,0:T(8,...) custom-call(s32[1]{0:T(128)} %bitcast.2.has_before, ...), custom_call_target="tpu_custom_call" | custom-call | flops 4000000000 | tf_op jit(solution)/shard_map/pallas_call | solution.py:409
  14.7 2.3 %collective-permute-done.vr_ref = bf16[512,256]{1,0:T(8,128)(2,1)S(1)} collective-permute-done((bf16[512,256]{1,0:T(8,128)(2,1)}, bf16[512,256]{1,0:T(8,128)(2,1)S(1)}, u32[]{:S(2)}, u32[]{:S(2)}) %collective-permute-start) | collective-permute-done | bytes 262176 | tf_op jit(solution)/shard_map/ppermute | solution.py:26
  17.0 0.0 copy-start
  17.0 0.0 copy-start.1
  17.0 2.9 %shard_map.120 = (f32[2,512,128]{2,1,0:T(8,128)S(1)}, f32[2,512,128]{2,1,0:T(8,128)S(1)}, bf16[512,256]{1,0:T(8,128)(2,1)S(1)}, bf16[32,8,128]{2,1,0:T(8,128)(2,1)}) custom-call(s32[1]{0:T(128)} %bitcast.2.has_before, bf16[512,256]{1,0:T(8,128)(2,1)S(1)} %collective-permute-done.vr_ref, f32[2,512,1024]{2,1,0:T(8,128)S(1)} %get-tuple-element.34.dd_ref, ...), custom_call_target="tpu_custom_call" | custom-call | flops 8000000000 | tf_op jit(solution)/shard_map/pallas_call | solution.py:409
  20.0 1.3 %collective-permute-start.2 = (bf16[512,256]{1,0:T(8,128)(2,1)S(1)}, bf16[512,256]{1,0:T(8,128)(2,1)S(1)}, u32[]{:S(2)}, u32[]{:S(2)}) collective-permute-start(bf16[512,256]{1,0:T(8,128)(2,1)S(1)} %get-tuple-element.51), channel_id=1, source_target_pairs={{4,0},{8,4},{12,8},{16,12},{20,16},{24,20},{28,24},{5,1},{9,5},{13... | collective-permute-start | bytes 786440 | tf_op jit(solution)/shard_map/ppermute | solution.py:26
  21.3 1.3 %collective-permute-start.3 = (bf16[512,256]{1,0:T(8,128)(2,1)S(1)}, bf16[512,256]{1,0:T(8,128)(2,1)S(1)}, u32[]{:S(2)}, u32[]{:S(2)}) collective-permute-start(bf16[512,256]{1,0:T(8,128)(2,1)S(1)} %get-tuple-element.52), channel_id=1, source_target_pairs={{4,0},{8,4},{12,8},{16,12},{20,16},{24,20},{28,24},{5,1},{9,5},{13... | collective-permute-start | bytes 786440 | tf_op jit(solution)/shard_map/ppermute | solution.py:26
  22.6 9.9 %all-to-all-start = ((bf16[32,8,128]{2,1,0:T(8,128)(2,1)}), bf16[32,8,128]{2,1,0:T(8,128)(2,1)S(1)}, u32[]{:S(2)}, u32[]{:S(2)}) async-start(bf16[32,8,128]{2,1,0:T(8,128)(2,1)} %get-tuple-element.56), calls=%async_computation | async-start | bytes 131072 | tf_op jit(solution)/shard_map/all_to_all | solution.py:478
  32.4 7.6 %all-to-all-done = bf16[32,8,128]{2,1,0:T(8,128)(2,1)S(1)} async-done(((bf16[32,8,128]{2,1,0:T(8,128)(2,1)}), bf16[32,8,128]{2,1,0:T(8,128)(2,1)S(1)}, u32[]{:S(2)}, u32[]{:S(2)}) %all-to-all-start) | async-done | bytes 65568 | tf_op jit(solution)/shard_map/all_to_all | solution.py:478
  40.1 0.7 %shard_map.122 = (f32[1,64]{1,0:T(1,128)}, f32[1,64]{1,0:T(1,128)}, f32[4,129]{1,0:T(4,128)}) custom-call(s32[1]{0:T(128)} %bitcast.3.tp_index, f32[8,128]{1,0:T(8,128)S(1)} %get-tuple-element.33.gains_ref, bf16[8,4,8,128]{3,2,1,0:T(8,128)(2,1)S(1)} %bitcast.7), custom_call_target="tpu_custom_call" | custom-call | flops 1000000 | tf_op jit(solution)/shard_map/pallas_call | solution.py:409
  40.8 0.0 collective-permute-done.2.dkb_ref
  40.8 0.0 collective-permute-done.3.dvb_ref
  40.8 0.0 copy-done
  40.8 0.0 copy-done.1
  40.8 1.8 %shard_map.121 = (bf16[512,256]{1,0:T(8,128)(2,1)}, bf16[512,256]{1,0:T(8,128)(2,1)}, bf16[512,256]{1,0:T(8,128)(2,1)}) custom-call(f32[8,128]{1,0:T(8,128)S(1)} %get-tuple-element.33.gains_ref, f32[2,512,128]{2,1,0:T(8,128)S(1)} %get-tuple-element.48.dqh_ref, bf16[512,256]{1,0:T(8,128)(2,1)S(1)} %copy-done, bf16[512,256]{1,0:T(8,128)(2,1)S(1)} %copy-done.1, ...), custom_call_target="tpu_custom_call" | custom-call | flops 1000000000 | tf_op jit(solution)/shard_map/pallas_call | solution.py:409
Async XLA Ops:
  0.6 11.9 %collective-permute-start.1 = (bf16[512,256]{1,0:T(8,128)(2,1)}, bf16[512,256]{1,0:T(8,128)(2,1)S(1)}, u32[]{:S(2)}, u32[]{:S(2)}) collective-permute-start(bf16[512,256]{1,0:T(8,128)(2,1)} %k_ref.1), channel_id=1, source_target_pairs={{0,4},{4,8},{8,12},{12,16},{16,20},{20,24},{24,28},{1,5},{5,9},{9,... | collective-permute-start | bytes 786440 | tf_op jit(solution)/shard_map/ppermute | solution.py:26
  5.6 11.5 %collective-permute-start = (bf16[512,256]{1,0:T(8,128)(2,1)}, bf16[512,256]{1,0:T(8,128)(2,1)S(1)}, u32[]{:S(2)}, u32[]{:S(2)}) collective-permute-start(bf16[512,256]{1,0:T(8,128)(2,1)} %v_hbm.1), channel_id=1, source_target_pairs={{0,4},{4,8},{8,12},{12,16},{16,20},{20,24},{24,28},{1,5},{5,9},{9,... | collective-permute-start | bytes 786440 | tf_op jit(solution)/shard_map/ppermute | solution.py:26
  17.0 23.8 %copy-start = (bf16[512,256]{1,0:T(8,128)(2,1)S(1)}, bf16[512,256]{1,0:T(8,128)(2,1)}, u32[]{:S(2)}) copy-start(bf16[512,256]{1,0:T(8,128)(2,1)} %q_ref.1) | copy-start | bytes 786436
  17.0 23.8 %copy-start.1 = (bf16[512,256]{1,0:T(8,128)(2,1)S(1)}, bf16[512,256]{1,0:T(8,128)(2,1)}, u32[]{:S(2)}) copy-start(bf16[512,256]{1,0:T(8,128)(2,1)} %k_ref.1) | copy-start | bytes 786436
  20.0 20.8 %collective-permute-start.2 = (bf16[512,256]{1,0:T(8,128)(2,1)S(1)}, bf16[512,256]{1,0:T(8,128)(2,1)S(1)}, u32[]{:S(2)}, u32[]{:S(2)}) collective-permute-start(bf16[512,256]{1,0:T(8,128)(2,1)S(1)} %get-tuple-element.51), channel_id=1, source_target_pairs={{4,0},{8,4},{12,8},{16,12},{20,16},{24,20},{28,24},{5,1},{9,5},{13... | collective-permute-start | bytes 786440 | tf_op jit(solution)/shard_map/ppermute | solution.py:26
  21.3 19.5 %collective-permute-start.3 = (bf16[512,256]{1,0:T(8,128)(2,1)S(1)}, bf16[512,256]{1,0:T(8,128)(2,1)S(1)}, u32[]{:S(2)}, u32[]{:S(2)}) collective-permute-start(bf16[512,256]{1,0:T(8,128)(2,1)S(1)} %get-tuple-element.52), channel_id=1, source_target_pairs={{4,0},{8,4},{12,8},{16,12},{20,16},{24,20},{28,24},{5,1},{9,5},{13... | collective-permute-start | bytes 786440 | tf_op jit(solution)/shard_map/ppermute | solution.py:26
  22.6 17.5 %all-to-all-start = ((bf16[32,8,128]{2,1,0:T(8,128)(2,1)}), bf16[32,8,128]{2,1,0:T(8,128)(2,1)S(1)}, u32[]{:S(2)}, u32[]{:S(2)}) async-start(bf16[32,8,128]{2,1,0:T(8,128)(2,1)} %get-tuple-element.56), calls=%async_computation | async-start | bytes 131072 | tf_op jit(solution)/shard_map/all_to_all | solution.py:478
